TPU v7x, 32 devices: a whole 2x2x4 slice. The times are simulated.
32 devices in a mesh: sp: 8 (over z, x), tp: 4 (over y, core).
Axes of the slice: x: 2, y: 2, z: 4, core: 2. Of those that a mesh axis runs over, the one named last changes fastest.
Arguments:
- inputs: bfloat16 [4096, 2048], P('sp', 'tp'), may hold values from -45 to 45
- norm_gain: float32 [3, 2048], replicated, may hold values from 0.1 to 1.9
- w_value: bfloat16 [3, 2048, 1024], P(None, 'sp', 'tp'), may hold values from -0.125 to 0.125
- w_gate: bfloat16 [3, 2048, 1024], P(None, 'sp', 'tp'), may hold values from -0.125 to 0.125
- conv_taps: float32 [3, 31, 1024], P(None, None, 'tp'), may hold values from -5 to 5
- ln_gain: float32 [3, 1024], P(None, 'tp'), may hold values from 0.1 to 1.9
- ln_bias: float32 [3, 1024], P(None, 'tp'), may hold values from -3 to 3
- w_out: bfloat16 [3, 1024, 2048], P(None, 'tp', 'sp'), may hold values from -0.1875 to 0.1875
Outputs:
- stream: bfloat16 [4096, 2048], P('sp', 'tp')
All inputs are finite; a program needn't handle non-finite values.
Results may differ from a plain program's by a relative error of at most 0.01.
Values may be sent and summed in bfloat16 or wider, within the bound.
A program may use at most 64 MiB of HBM per device.

v0:
```python
import functools

import jax
import jax.numpy as jnp
from jax import lax
from jax.experimental import pallas as pl
from jax.experimental.pallas import tpu as pltpu
from jax.sharding import PartitionSpec as P

MESH = pl.DeviceIdType.MESH
PAIR = 2
CHUNK = 128
HALO = 32
LANES = 128
FIRST = 6
Z_AHEAD, X_AHEAD = 1, 2
STEPS = (0, 1, 2, 4, 5, 6, 7, 8, 8)
SIDE = (1,)


def fused_kernel(
    n_sp, n_tp, eps,
    x_ref, gain_ref, wv_ref, wg_ref, taps_ref, lng_ref, lnb_ref, wo_ref,
    out_ref,
    wv_all, wg_all, wo_all, xf, hid, glu, filt, rim_out, rim_in, stat,
    ps_out, ps_in, keep, fs_out, fs_in,
    w_recv, w_zsend, w_xsend, ag_recv, ag_send, rim_s, rim_r, st_recv, st_send,
    ps_s, ps_r, fs_s, fs_r,
):
    sp = lax.axis_index("sp")
    tp = lax.axis_index("tp")
    layers, depth = wv_ref.shape[0], wv_ref.shape[1]
    rows, dblk = x_ref.shape
    width = wo_ref.shape[2]
    chan = wv_ref.shape[2]
    taps = taps_ref.shape[1]
    features = dblk * n_tp
    channels = chan * n_tp
    n_chunks = rows // CHUNK
    n_out = n_sp // PAIR
    per_blk = dblk // width
    outer, inner = lax.div(sp, PAIR), lax.rem(sp, PAIR)
    x_peer = outer * PAIR + (PAIR - 1 - inner)
    far_half, core = lax.div(tp, PAIR), lax.rem(tp, PAIR)
    partner = far_half * PAIR + (PAIR - 1 - core)
    far = (n_tp // PAIR - 1 - far_half) * PAIR + core
    far_partner = (n_tp // PAIR - 1 - far_half) * PAIR + (PAIR - 1 - core)
    first_off = HALO - (taps - 1)
    halves = chan // LANES

    barrier = pltpu.get_barrier_semaphore()
    for step in range(1, n_sp):
        pl.semaphore_signal(barrier, inc=1, device_id=(lax.rem(sp + step, n_sp), tp), device_id_type=MESH)
    for step in range(1, n_tp):
        pl.semaphore_signal(barrier, inc=1, device_id=(sp, lax.rem(tp + step, n_tp)), device_id_type=MESH)
    xf[tp] = x_ref[...]

    def own_weights(l, carry):
        own = pl.ds(pl.multiple_of(sp * depth, depth), depth)
        wv_all[l, own, :] = wv_ref[l]
        wg_all[l, own, :] = wg_ref[l]
        wo_all[l, sp] = wo_ref[l]
        return carry

    lax.fori_loop(0, layers, own_weights, 0)
    pl.semaphore_wait(barrier, n_sp - 1 + n_tp - 1)

    def chunk_rows(c):
        return pl.ds(pl.multiple_of(c * CHUNK, CHUNK), CHUNK)

    def remote(src, dst, send, recv, sp_to, tp_to):
        return pltpu.make_async_remote_copy(
            src_ref=src, dst_ref=dst, send_sem=send, recv_sem=recv,
            device_id=(sp_to, tp_to), device_id_type=MESH,
        )

    w_in = (wv_ref, wg_ref, wo_ref)

    def w_slot(m, l, s):
        if m == 2:
            return wo_all.at[l, s]
        return (wv_all, wg_all)[m].at[l, pl.ds(pl.multiple_of(s * depth, depth), depth), :]

    last = n_out - 1
    upper = lax.div(outer, n_out // 2)
    near_end = outer + upper * (last - 2 * outer)

    def line(j):
        near = j + 1 - (near_end if j == 0 else 0)
        return near + upper * (last - 2 * near)

    def z_copy(m, l, j):
        to = line(j) * PAIR + inner
        return remote(w_in[m].at[l], w_slot(m, l, sp), w_zsend.at[l, m, j], w_recv.at[l, m, sp], to, tp)

    def z_arrival(m, l, j):
        s = line(j) * PAIR + inner
        return remote(w_in[m].at[l], w_slot(m, l, s), w_zsend.at[l, m, j], w_recv.at[l, m, s], s, tp)

    def z_forward(m, l):
        s = line(last - 1) * PAIR + inner
        to = upper * last * PAIR + inner
        slot = w_slot(m, l, s)
        return remote(slot, slot, w_zsend.at[l, m, last], w_recv.at[l, m, s], to, tp)

    def x_own(m, l):
        return remote(w_in[m].at[l], w_slot(m, l, sp), w_xsend.at[l, m, last], w_recv.at[l, m, sp], x_peer, tp)

    def x_copy(m, l, j):
        s = line(j) * PAIR + inner
        slot = w_slot(m, l, s)
        return remote(slot, slot, w_xsend.at[l, m, j], w_recv.at[l, m, s], x_peer, tp)

    def x_arrival(m, l, z):
        s = z * PAIR + (PAIR - 1 - inner)
        slot = w_slot(m, l, s)
        return remote(slot, slot, w_xsend.at[l, m, last], w_recv.at[l, m, s], x_peer, tp)

    def side_copy(m, l):
        to = line(0) * PAIR + inner
        slot = w_slot(m, l, x_peer)
        return remote(slot, slot, w_xsend.at[l, m, 0], w_recv.at[l, m, x_peer], to, tp)

    def z_send_all(m, l):
        for j in range(last - 1):
            z_copy(m, l, j).start()

        @pl.when(near_end == 1)
        def _():
            z_copy(m, l, last - 1).start()

    def relay_piece(m, l, j):
        z_arrival(m, l, j).wait_recv()
        if j == 0 and m in SIDE:
            x_arrival(m, l, outer).wait_recv()
            side_copy(m, l).start()
        else:
            x_copy(m, l, j).start()
        if j == last - 1:
            @pl.when(near_end == 1)
            def _():
                z_forward(m, l).start()

    def relay(m, l):
        for j in range(last):
            relay_piece(m, l, j)

    def w_ready(m, l):
        if m not in SIDE:
            x_arrival(m, l, outer).wait_recv()
        for j in range(last):
            x_arrival(m, l, line(j)).wait_recv()

    def ag_far(c):
        r = chunk_rows(c)
        return remote(xf.at[tp, r, :], xf.at[tp, r, :], ag_send.at[0, c], ag_recv.at[0, c], sp, far)

    def ag_partner(c):
        r = chunk_rows(c)
        return remote(xf.at[tp, r, :], xf.at[tp, r, :], ag_send.at[1, c], ag_recv.at[1, c], sp, partner)

    def ag_forward(c):
        r = chunk_rows(c)
        return remote(xf.at[far, r, :], xf.at[far, r, :], ag_send.at[2, c], ag_recv.at[2, c], sp, partner)

    def stat_copy(l, c, step):
        to = lax.rem(tp + step, n_tp)
        return remote(stat.at[l, c, tp], stat.at[l, c, tp], st_send.at[c, step], st_recv.at[c, tp], sp, to)

    def stat_arrival(l, c, step):
        src = lax.rem(tp + step, n_tp)
        return remote(stat.at[l, c, src], stat.at[l, c, src], st_send.at[c, step], st_recv.at[c, src], sp, src)

    def ps_copy(c):
        r = chunk_rows(c)
        return remote(ps_out.at[:, r, :], ps_in.at[:, r, :], ps_s.at[c], ps_r.at[c], sp, partner)

    def fs_copy(c):
        r = chunk_rows(c)
        return remote(fs_out.at[r, :], fs_in.at[r, :], fs_s.at[c], fs_r.at[c], sp, far)

    def rim_copy(l):
        to = lax.rem(sp + 1, n_sp)
        return remote(rim_out.at[l], rim_in.at[l], rim_s.at[l], rim_r.at[l], to, tp)

    for c in range(n_chunks):
        ag_far(c).start()
        ag_partner(c).start()
    for q in range(Z_AHEAD):
        z_send_all(q % 3, q // 3)
    for q in range(X_AHEAD):
        x_own(q % 3, q // 3).start()
    for p in range(FIRST):
        q, j = divmod(p, last)
        if j == 0:
            z_send_all((q + Z_AHEAD) % 3, (q + Z_AHEAD) // 3)
            x_own((q + X_AHEAD) % 3, (q + X_AHEAD) // 3).start()
        relay_piece(q % 3, q // 3, j)

    def do_glu(l, c):
        ag_partner(c).wait_recv()
        ag_forward(c).wait_recv()
        r = chunk_rows(c)
        blocks = [xf[b, r, :].astype(jnp.float32) for b in range(n_tp)]
        total = sum(jnp.sum(b * b, axis=1, keepdims=True) for b in blocks)
        scale = lax.rsqrt(total / features + eps)
        for b in range(n_tp):
            cols = slice(b * dblk, (b + 1) * dblk)
            hid[:, cols] = (xf[b, r, :].astype(jnp.float32) * scale * gain_ref[pl.ds(l, 1), cols]).astype(jnp.bfloat16)
        h = hid[...]
        value = jnp.dot(h, wv_all[l], preferred_element_type=jnp.float32)
        gate = jnp.dot(h, wg_all[l], preferred_element_type=jnp.float32)
        g = (value * jax.nn.sigmoid(gate)).astype(jnp.bfloat16)
        for k in range(halves):
            glu[k, pl.ds(pl.multiple_of(HALO + c * CHUNK, HALO), CHUNK), :] = g[:, k * LANES:(k + 1) * LANES].astype(jnp.float32)

        @pl.when((c == n_chunks - 1) & (sp < n_sp - 1))
        def _():
            rim_out[l] = g[CHUNK - HALO:, :]
            rim_copy(l).start()

    def do_conv(l, c):
        @pl.when((c == 0) & (sp > 0))
        def _():
            rim_copy(l).wait_recv()
            rim = rim_in[l].astype(jnp.float32)
            for k in range(halves):
                glu[k, 0:HALO, :] = rim[:, k * LANES:(k + 1) * LANES]

        @pl.when((c == 0) & (sp == 0))
        def _():
            glu[:, 0:HALO, :] = jnp.zeros((halves, HALO, LANES), jnp.float32)

        r = chunk_rows(c)
        sums = jnp.zeros((CHUNK, 1), jnp.float32)
        squares = jnp.zeros((CHUNK, 1), jnp.float32)
        for k in range(halves):
            acc = jnp.zeros((CHUNK, LANES), jnp.float32)
            for tap in range(taps):
                acc = acc + taps_ref[l, tap:tap + 1, k * LANES:(k + 1) * LANES] * glu[
                    k, pl.ds(c * CHUNK + first_off + tap, CHUNK), :]
            filt[r, k * LANES:(k + 1) * LANES] = acc
            sums = sums + jnp.sum(acc, axis=1, keepdims=True)
            squares = squares + jnp.sum(acc * acc, axis=1, keepdims=True)
        lane = lax.broadcasted_iota(jnp.int32, (CHUNK, LANES), 1)
        both = jnp.where(lane == 0, sums, squares)
        stat[l, c, tp] = jnp.transpose(both)[0:8, :]
        for step in range(1, n_tp):
            stat_copy(l, c, step).start()

    def do_out(l, c):
        for step in range(1, n_tp):
            stat_arrival(l, c, step).wait_recv()
        r = chunk_rows(c)
        tot = stat[l, c, 0]
        for b in range(1, n_tp):
            tot = tot + stat[l, c, b]
        tot = jnp.transpose(jnp.concatenate([tot, jnp.zeros((LANES - 8, CHUNK), jnp.float32)], axis=0))
        mean = tot[:, 0:1] / channels
        var = tot[:, 1:2] / channels - mean * mean
        pre = (filt[r, :] - mean) * lax.rsqrt(var + eps) * lng_ref[pl.ds(l, 1), :] + lnb_ref[pl.ds(l, 1), :]
        normed = jax.nn.silu(pre).astype(jnp.bfloat16)
        for step in range(1, n_tp):
            stat_copy(l, c, step).wait_send()
        ag_far(c).wait_send()
        ag_partner(c).wait_send()
        ag_forward(c).wait_send()
        for half in range(n_tp // PAIR):
            for q in range(per_blk):
                cols = slice(q * width, (q + 1) * width)
                away = (half * PAIR + (PAIR - 1 - core)) * per_blk + q
                ps_out[half, r, cols] = jnp.dot(
                    normed, wo_all[l, away], preferred_element_type=jnp.float32).astype(jnp.bfloat16)
        ps_copy(c).start()
        for half in range(n_tp // PAIR):
            for q in range(per_blk):
                cols = slice(q * width, (q + 1) * width)
                mine = (half * PAIR + core) * per_blk + q
                keep[half, r, cols] = jnp.dot(normed, wo_all[l, mine], preferred_element_type=jnp.float32)

    def do_pair(l, c):
        ps_copy(c).wait_recv()
        r = chunk_rows(c)
        other = n_tp // PAIR - 1 - far_half
        fs_out[r, :] = (keep[other, r, :] + ps_in[other, r, :].astype(jnp.float32)).astype(jnp.bfloat16)
        fs_copy(c).start()

    def do_final(l, c):
        fs_copy(c).wait_recv()
        ps_copy(c).wait_send()
        fs_copy(c).wait_send()
        r = chunk_rows(c)
        branch = keep[far_half, r, :] + ps_in[far_half, r, :].astype(jnp.float32) + fs_in[r, :].astype(jnp.float32)
        new = (xf[tp, r, :].astype(jnp.float32) + branch).astype(jnp.bfloat16)

        @pl.when(l < layers - 1)
        def _():
            xf[tp, r, :] = new
            ag_far(c).start()
            ag_partner(c).start()

        @pl.when(l == layers - 1)
        def _():
            out_ref[r, :] = new

    def layer_body(l, carry):
        base = lax.rem(l, n_chunks)
        more = l < layers - 1

        def step_body(i, inner_carry):
            def at(back):
                return lax.rem(base + i + n_chunks * 2 - back, n_chunks)

            for k in range(3 * last):
                q, j = divmod(FIRST + k, last)
                if j == 0:
                    z_next, x_next = q + Z_AHEAD, q + X_AHEAD

                    @pl.when((i == STEPS[k]) & (l + z_next // 3 < layers))
                    def _():
                        z_send_all(z_next % 3, l + z_next // 3)

                    @pl.when((i == STEPS[k]) & (l + x_next // 3 < layers))
                    def _():
                        x_own(x_next % 3, l + x_next // 3).start()

                @pl.when((i == STEPS[k]) & (l + q // 3 < layers))
                def _():
                    relay_piece(q % 3, l + q // 3, j)

            @pl.when(i < n_chunks)
            def _():
                ag_far(at(0)).wait_recv()
                ag_forward(at(0)).start()

            @pl.when(i == 0)
            def _():
                w_ready(0, l)
                w_ready(1, l)

            @pl.when((i >= 2) & (i < n_chunks + 2))
            def _():
                do_conv(l, at(1))

            @pl.when(i < n_chunks)
            def _():
                do_glu(l, at(0))

            @pl.when(i == 3)
            def _():
                w_ready(2, l)

            @pl.when((i >= 3) & (i < n_chunks + 3))
            def _():
                do_out(l, at(2))

            @pl.when((i >= 4) & (i < n_chunks + 4))
            def _():
                do_pair(l, at(3))

            @pl.when(i >= 5)
            def _():
                do_final(l, at(4))

            return inner_carry

        lax.fori_loop(0, n_chunks + 5, step_body, 0)

        return carry

    lax.fori_loop(0, layers, layer_body, 0)

    def drain(l, carry):
        for m in range(3):
            for j in range(last - 1):
                z_copy(m, l, j).wait_send()

            @pl.when(near_end == 1)
            def _():
                z_copy(m, l, last - 1).wait_send()
                z_forward(m, l).wait_send()

            for j in range(last):
                (side_copy(m, l) if j == 0 and m in SIDE else x_copy(m, l, j)).wait_send()
            x_own(m, l).wait_send()

        @pl.when(sp < n_sp - 1)
        def _():
            rim_copy(l).wait_send()

        return carry

    lax.fori_loop(0, layers, drain, 0)


def fused_shards(n_sp, n_tp, inputs, norm_gain, w_value, w_gate, conv_taps, ln_gain, ln_bias, w_out):
    layers, depth, chan = w_value.shape
    rows, dblk = inputs.shape
    width = w_out.shape[2]
    n_chunks = rows // CHUNK
    features = dblk * n_tp
    n_half = n_tp // PAIR
    bf16, f32 = jnp.bfloat16, jnp.float32
    dma = pltpu.SemaphoreType.DMA
    vmem = pl.BlockSpec(memory_space=pltpu.VMEM)
    return pl.pallas_call(
        functools.partial(fused_kernel, n_sp, n_tp, 1e-06),
        out_shape=jax.ShapeDtypeStruct((rows, dblk), bf16),
        in_specs=[vmem] * 8,
        out_specs=vmem,
        scratch_shapes=[
            pltpu.VMEM((layers, n_sp * depth, chan), bf16),
            pltpu.VMEM((layers, n_sp * depth, chan), bf16),
            pltpu.VMEM((layers, n_sp, chan, width), bf16),
            pltpu.VMEM((n_tp, rows, dblk), bf16),
            pltpu.VMEM((CHUNK, features), bf16),
            pltpu.VMEM((chan // LANES, HALO + rows, LANES), f32),
            pltpu.VMEM((rows, chan), f32),
            pltpu.VMEM((layers, HALO, chan), bf16),
            pltpu.VMEM((layers, HALO, chan), bf16),
            pltpu.VMEM((layers, n_chunks, n_tp, 8, CHUNK), f32),
            pltpu.VMEM((n_half, rows, dblk), bf16),
            pltpu.VMEM((n_half, rows, dblk), bf16),
            pltpu.VMEM((n_half, rows, dblk), f32),
            pltpu.VMEM((rows, dblk), bf16),
            pltpu.VMEM((rows, dblk), bf16),
            dma((layers, 3, n_sp)),
            dma((layers, 3, n_sp // PAIR)),
            dma((layers, 3, n_sp // PAIR)),
            dma((3, n_chunks)),
            dma((3, n_chunks)),
            dma((layers,)),
            dma((layers,)),
            dma((n_chunks, n_tp)),
            dma((n_chunks, n_tp)),
            dma((n_chunks,)),
            dma((n_chunks,)),
            dma((n_chunks,)),
            dma((n_chunks,)),
        ],
        compiler_params=pltpu.CompilerParams(collective_id=0, has_side_effects=True),
    )(
        inputs,
        norm_gain,
        w_value,
        w_gate,
        conv_taps,
        ln_gain,
        ln_bias,
        w_out,
    )


def fits_kernel(n_sp, n_tp, inputs, w_value, conv_taps, w_out):
    rows, dblk = inputs.shape
    width = w_out.shape[2]
    return (
        n_sp == 4 * PAIR
        and n_tp == PAIR * PAIR
        and rows % CHUNK == 0
        and rows // CHUNK >= 4
        and w_value.shape[0] >= 2
        and w_value.shape[1] % LANES == 0
        and w_value.shape[2] % LANES == 0
        and width % LANES == 0
        and dblk % width == 0
        and conv_taps.shape[1] - 1 <= HALO
    )


def shards(inputs, norm_gain, w_value, w_gate, conv_taps, ln_gain, ln_bias, w_out):
    n_sp, n_tp = lax.axis_size("sp"), lax.axis_size("tp")
    args = (inputs, norm_gain, w_value, w_gate, conv_taps, ln_gain, ln_bias, w_out)
    if fits_kernel(n_sp, n_tp, inputs, w_value, conv_taps, w_out):
        return fused_shards(n_sp, n_tp, *args)
    return plain_shards(*args)


def from_behind(block, axis, distance):
    devices = range(lax.axis_size(axis))
    route = [(i - distance, i) for i in devices if i - distance in devices]
    return lax.ppermute(block, axis, route)


def plain_shards(inputs, norm_gain, w_value, w_gate, conv_taps, ln_gain, ln_bias, w_out):
    rows = inputs.shape[0]
    reach = conv_taps.shape[1] - 1
    layers = conv_taps.shape[0]
    channels = conv_taps.shape[2] * lax.axis_size("tp")
    whole_value, whole_gate, whole_out = (
        lax.all_gather(w_value, "sp", axis=1, tiled=True),
        lax.all_gather(w_gate, "sp", axis=1, tiled=True),
        lax.all_gather(w_out, "sp", axis=2, tiled=True),
    )
    stream = inputs
    for layer in range(layers):
        full_rows = lax.all_gather(stream, "tp", axis=1, tiled=True)
        xf = full_rows.astype(jnp.float32)
        meansq = jnp.mean(xf * xf, axis=1, keepdims=True)
        hidden = (xf * lax.rsqrt(meansq + 1e-06) * norm_gain[layer][None, :]).astype(jnp.bfloat16)
        value = jnp.dot(hidden, whole_value[layer], preferred_element_type=jnp.float32)
        gate = jnp.dot(hidden, whole_gate[layer], preferred_element_type=jnp.float32)
        glu = (value * jax.nn.sigmoid(gate)).astype(jnp.bfloat16)
        rim = from_behind(glu[rows - reach :], "sp", 1)
        padded = jnp.concatenate([rim, glu], axis=0)
        count = padded.shape[0] - reach
        filtered = jnp.zeros((count, glu.shape[1]), jnp.float32)
        for tap in range(reach + 1):
            filtered = filtered + conv_taps[layer, tap][None, :] * padded[tap : tap + count].astype(
                jnp.float32
            )
        total_sum, total_sq = lax.psum(
            (jnp.sum(filtered, axis=1), jnp.sum(filtered * filtered, axis=1)), "tp"
        )
        mean_val = (total_sum / channels)[:, None]
        var_val = (total_sq / channels)[:, None] - mean_val * mean_val
        normed = jax.nn.silu(
            (filtered - mean_val) * lax.rsqrt(var_val + 1e-06) * ln_gain[layer][None, :]
            + ln_bias[layer][None, :]
        ).astype(jnp.bfloat16)
        partial_out = jnp.dot(normed, whole_out[layer], preferred_element_type=jnp.float32)
        summed = lax.psum_scatter(
            partial_out.astype(jnp.bfloat16), "tp", scatter_dimension=1, tiled=True
        ).astype(jnp.float32)
        kept = stream.astype(jnp.float32)
        stream = (kept + summed).astype(jnp.bfloat16)
    return stream


def solution(mesh):
    in_specs = (
        P("sp", "tp"),
        P(),
        P(None, "sp", "tp"),
        P(None, "sp", "tp"),
        P(None, None, "tp"),
        P(None, "tp"),
        P(None, "tp"),
        P(None, "tp", "sp"),
    )
    out_specs = P("sp", "tp")
    return jax.shard_map(shards, mesh=mesh, in_specs=in_specs, out_specs=out_specs, check_vma=False)
```

profile of v0, /device:TPU:3, one launch (start us, length us, event | category | flops | bytes accessed | tf_op | source)
XLA Modules:
  0.0 134.4 jit_solution(2052734988583237710)
XLA Ops:
  0.0 132.5 %shard_map.82 = bf16[512,512]{1,0:T(8,128)(2,1)} custom-call(bf16[512,512]{1,0:T(8,128)(2,1)} %x_ref.1, f32[3,2048]{1,0:T(4,128)} %gain_ref.1, bf16[3,256,256]{2,1,0:T(8,128)(2,1)} %wv_ref.1, bf16[3,256,256]{2,1,0:T(8,128)(2,1)} %wg_ref.1, f32[3,31,256]{2,1,0:T(8,128)} %taps_ref.1, f32[3,256]{1,0:T(4,128)} %lng_ref.1, f32[3,256]{1,0:T(4,128)} %lnb_ref.1, ...), custom_call_target="tpu_custom_call" | custom-call | tf_op jit(solution)/shard_map/pallas_call | solution.py:406
  132.6 1.9 %copy.10 = bf16[512,512]{1,0:T(8,128)(2,1)} copy(bf16[512,512]{1,0:T(8,128)(2,1)} %shard_map.82) | data formatting | bytes 1048576
where the time goes:
time: 137 us; the launch traced here: 134 us
  Pallas kernels  133 us (97%)
  local copies, waits for them, and re-layouts  1.87 us (1%)
    pallas_call x1, Pallas kernels, fused_shards(): pl.pallas_call(functools.partial(fused_kernel, n_sp, n_tp, 1e-06), out_sh...  133 us

commit v1 on v0

--- a/solution.py
+++ b/solution.py
@@ -12,20 +12,52 @@
 CHUNK = 128
 HALO = 32
 LANES = 128
-FIRST = 6
-Z_AHEAD, X_AHEAD = 1, 2
-STEPS = (0, 1, 2, 4, 5, 6, 7, 8, 8)
-SIDE = (1,)
+V, G, O, UP, OVER, ZOWN, XOWN = 0, 1, 2, 3, 4, 5, 6
+OWN_X = ((XOWN, V, 1), (XOWN, G, 1))
+OWN_Z = ((ZOWN, V, 1), (ZOWN, G, 1))
+
+
+def every(kind, later):
+    return tuple((kind, j, later) for j in range(4))
+
+
+END_OPEN = (
+    (V, 0, 0), *OWN_Z, (G, 0, 0), (V, 1, 0), (G, 1, 0), (V, 2, 0), (G, 2, 0), *OWN_X, (O, 0, 0),
+)
+HEAD_OPEN = (
+    (V, 0, 0), *every(UP, 0), *OWN_Z, (G, 0, 0), (V, 1, 0), (G, 1, 0), (V, 2, 0), (G, 2, 0), *OWN_X, *every(OVER, 0),
+)
+MID_OPEN = (
+    (V, 0, 0), (V, 1, 0), (G, 0, 0), (G, 1, 0), (V, 2, 0), (G, 2, 0), *OWN_X, (ZOWN, V, 1), *every(O, 0), (ZOWN, G, 1),
+)
+NEXT_OPEN = MID_OPEN
+END_PLAN = {
+    1: ((O, 1, 0),), 2: ((O, 2, 0),), 3: ((O, 3, 0),), 4: ((V, 0, 1),), 5: ((V, 1, 1), (ZOWN, V, 2), (ZOWN, G, 2)),
+    6: ((V, 2, 1),), 7: ((G, 0, 1),), 8: ((G, 1, 1),), 9: ((G, 2, 1), (XOWN, V, 2), (XOWN, G, 2)), 12: ((O, 0, 1),),
+}
+HEAD_PLAN = {
+    3: every(UP, 1), 4: ((V, 0, 1),), 5: ((V, 1, 1), (ZOWN, V, 2), (ZOWN, G, 2)), 6: ((V, 2, 1),),
+    7: ((G, 0, 1),), 8: ((G, 1, 1),), 9: ((G, 2, 1), (XOWN, V, 2), (XOWN, G, 2), *every(OVER, 1)),
+}
+MID_PLAN = {
+    1: ((V, 0, 1),), 2: ((V, 1, 1),), 3: ((V, 2, 1),), 4: ((G, 0, 1),), 5: ((G, 1, 1),),
+    6: ((G, 2, 1), (XOWN, V, 2), (XOWN, G, 2), (ZOWN, V, 2)),
+    9: ((O, 0, 1),), 10: ((O, 1, 1),), 11: ((O, 2, 1),), 12: ((O, 3, 1), (ZOWN, G, 2)),
+}
+NEXT_PLAN = {
+    1: ((V, 0, 1),), 2: ((V, 1, 1),), 3: ((V, 2, 1),), 4: ((G, 0, 1), (UP, 0, 1)), 5: ((G, 1, 1), (UP, 1, 1)),
+    6: ((G, 2, 1), (UP, 2, 1), (XOWN, V, 2), (XOWN, G, 2), (ZOWN, V, 2)), 7: ((UP, 3, 1),),
+    8: (*every(OVER, 1), (ZOWN, G, 2)),
+}
 
 
 def fused_kernel(
     n_sp, n_tp, eps,
     x_ref, gain_ref, wv_ref, wg_ref, taps_ref, lng_ref, lnb_ref, wo_ref,
     out_ref,
-    wv_all, wg_all, wo_all, xf, hid, glu, filt, rim_out, rim_in, stat,
-    ps_out, ps_in, keep, fs_out, fs_in,
-    w_recv, w_zsend, w_xsend, ag_recv, ag_send, rim_s, rim_r, st_recv, st_send,
-    ps_s, ps_r, fs_s, fs_r,
+    wv_all, wg_all, wo_all, xf, hid, glu, filt, rim_out, rim_in, stat, nrm,
+    w_recv, w_zsend, w_xsend, o_recv, o_send, og_send,
+    ag_recv, ag_send, rim_s, rim_r, st_recv, st_send, nr_recv, nr_send,
 ):
     sp = lax.axis_index("sp")
     tp = lax.axis_index("tp")
@@ -38,32 +70,62 @@
     channels = chan * n_tp
     n_chunks = rows // CHUNK
     n_out = n_sp // PAIR
-    per_blk = dblk // width
     outer, inner = lax.div(sp, PAIR), lax.rem(sp, PAIR)
     x_peer = outer * PAIR + (PAIR - 1 - inner)
     far_half, core = lax.div(tp, PAIR), lax.rem(tp, PAIR)
     partner = far_half * PAIR + (PAIR - 1 - core)
     far = (n_tp // PAIR - 1 - far_half) * PAIR + core
-    far_partner = (n_tp // PAIR - 1 - far_half) * PAIR + (PAIR - 1 - core)
     first_off = HALO - (taps - 1)
     halves = chan // LANES
 
+    last = n_out - 1
+    upper = lax.div(outer, n_out // 2)
+    near_end = outer + upper * (last - 2 * outer)
+
+    def line(j):
+        near = j + 1 - (near_end if j == 0 else 0)
+        return near + upper * (last - 2 * near)
+
+    slant = sp + 2 * inner - 1
+    has_slant = (slant >= 0) & (slant < n_sp)
     barrier = pltpu.get_barrier_semaphore()
-    for step in range(1, n_sp):
-        pl.semaphore_signal(barrier, inc=1, device_id=(lax.rem(sp + step, n_sp), tp), device_id_type=MESH)
+
+    def greet(sp_to, tp_to):
+        pl.semaphore_signal(barrier, inc=1, device_id=(sp_to, tp_to), device_id_type=MESH)
+
+    greet(line(0) * PAIR + inner, tp)
+    greet(x_peer, tp)
     for step in range(1, n_tp):
-        pl.semaphore_signal(barrier, inc=1, device_id=(sp, lax.rem(tp + step, n_tp)), device_id_type=MESH)
+        greet(sp, lax.rem(tp + step, n_tp))
+
+    @pl.when(near_end == 1)
+    def _():
+        greet(line(1) * PAIR + inner, tp)
+
+    @pl.when(has_slant)
+    def _():
+        greet(slant, tp)
+
     xf[tp] = x_ref[...]
 
+    def own_rows(s):
+        return pl.ds(pl.multiple_of(s * depth, depth), depth)
+
+    def o_slot(l, x, b):
+        return wo_all.at[l, x, pl.ds(pl.multiple_of(b * chan, chan), chan), :]
+
     def own_weights(l, carry):
-        own = pl.ds(pl.multiple_of(sp * depth, depth), depth)
-        wv_all[l, own, :] = wv_ref[l]
-        wg_all[l, own, :] = wg_ref[l]
-        wo_all[l, sp] = wo_ref[l]
+        wv_all[l, own_rows(sp), :] = wv_ref[l]
+        wg_all[l, own_rows(sp), :] = wg_ref[l]
+
+        @pl.when(outer == tp)
+        def _():
+            wo_all[l, inner, pl.ds(pl.multiple_of(tp * chan, chan), chan), :] = wo_ref[l]
+
         return carry
 
     lax.fori_loop(0, layers, own_weights, 0)
-    pl.semaphore_wait(barrier, n_sp - 1 + n_tp - 1)
+    pl.semaphore_wait(barrier, 2 + n_tp - 1 + near_end + has_slant.astype(jnp.int32))
 
     def chunk_rows(c):
         return pl.ds(pl.multiple_of(c * CHUNK, CHUNK), CHUNK)
@@ -74,20 +136,10 @@
             device_id=(sp_to, tp_to), device_id_type=MESH,
         )
 
-    w_in = (wv_ref, wg_ref, wo_ref)
+    w_in = (wv_ref, wg_ref)
 
     def w_slot(m, l, s):
-        if m == 2:
-            return wo_all.at[l, s]
-        return (wv_all, wg_all)[m].at[l, pl.ds(pl.multiple_of(s * depth, depth), depth), :]
-
-    last = n_out - 1
-    upper = lax.div(outer, n_out // 2)
-    near_end = outer + upper * (last - 2 * outer)
-
-    def line(j):
-        near = j + 1 - (near_end if j == 0 else 0)
-        return near + upper * (last - 2 * near)
+        return (wv_all, wg_all)[m].at[l, own_rows(s), :]
 
     def z_copy(m, l, j):
         to = line(j) * PAIR + inner
@@ -97,11 +149,11 @@
         s = line(j) * PAIR + inner
         return remote(w_in[m].at[l], w_slot(m, l, s), w_zsend.at[l, m, j], w_recv.at[l, m, s], s, tp)
 
-    def z_forward(m, l):
-        s = line(last - 1) * PAIR + inner
-        to = upper * last * PAIR + inner
+    def z_forward(m, l, j):
+        s = line(j) * PAIR + inner
+        to = line(1 if j == 0 else 0) * PAIR + inner
         slot = w_slot(m, l, s)
-        return remote(slot, slot, w_zsend.at[l, m, last], w_recv.at[l, m, s], to, tp)
+        return remote(slot, slot, w_zsend.at[l, m, PAIR + j], w_recv.at[l, m, s], to, tp)
 
     def x_own(m, l):
         return remote(w_in[m].at[l], w_slot(m, l, sp), w_xsend.at[l, m, last], w_recv.at[l, m, sp], x_peer, tp)
@@ -121,36 +173,84 @@
         slot = w_slot(m, l, x_peer)
         return remote(slot, slot, w_xsend.at[l, m, 0], w_recv.at[l, m, x_peer], to, tp)
 
-    def z_send_all(m, l):
-        for j in range(last - 1):
-            z_copy(m, l, j).start()
+    def z_own(m, l):
+        z_copy(m, l, 0).start()
 
         @pl.when(near_end == 1)
         def _():
-            z_copy(m, l, last - 1).start()
-
-    def relay_piece(m, l, j):
+            z_copy(m, l, 1).start()
+
+    def relay_piece(m, l, j, side):
         z_arrival(m, l, j).wait_recv()
-        if j == 0 and m in SIDE:
+
+        @pl.when(near_end == 1)
+        def _():
+            z_forward(m, l, j).start()
+
+        if j == 0 and side:
             x_arrival(m, l, outer).wait_recv()
             side_copy(m, l).start()
         else:
             x_copy(m, l, j).start()
-        if j == last - 1:
-            @pl.when(near_end == 1)
+
+    def w_ready(m, l):
+        if m == 1:
+            @pl.when(l == 0)
             def _():
-                z_forward(m, l).start()
-
-    def relay(m, l):
-        for j in range(last):
-            relay_piece(m, l, j)
-
-    def w_ready(m, l):
-        if m not in SIDE:
+                x_arrival(m, l, outer).wait_recv()
+        else:
             x_arrival(m, l, outer).wait_recv()
         for j in range(last):
             x_arrival(m, l, line(j)).wait_recv()
 
+    def o_gather(l):
+        return remote(wo_ref.at[l], o_slot(l, inner, tp), og_send.at[l], o_recv.at[l, tp, inner], sp, outer)
+
+    def o_hop(l, j, way, to):
+        b = lax.rem(tp + j, n_tp)
+        slot = o_slot(l, inner, b)
+        return remote(slot, slot, o_send.at[l, j, way], o_recv.at[l, b, inner], to, tp)
+
+    def o_arrival(l, b, x):
+        slot = o_slot(l, x, b)
+        return remote(slot, slot, o_send.at[l, 0, 0], o_recv.at[l, b, x], x_peer, tp)
+
+    goes_up = (outer >= tp) & (outer < last)
+    goes_down = (outer <= tp) & (outer > 0)
+
+    def send_o(l):
+        @pl.when(outer != tp)
+        def _():
+            o_gather(l).start()
+
+    def o_arrived(l, j):
+        if j == 0:
+            @pl.when(outer != tp)
+            def _():
+                o_arrival(l, tp, inner).wait_recv()
+        else:
+            o_arrival(l, lax.rem(tp + j, n_tp), inner).wait_recv()
+
+    def o_along(l, j):
+        @pl.when(goes_up)
+        def _():
+            o_hop(l, j, 0, sp + PAIR).start()
+
+        @pl.when(goes_down)
+        def _():
+            o_hop(l, j, 1, sp - PAIR).start()
+
+    def relay_o(l, j, kind):
+        if kind != OVER:
+            o_arrived(l, j)
+            o_along(l, j)
+        if kind != UP:
+            o_hop(l, j, 2, x_peer).start()
+
+    def o_ready(l):
+        for j in range(n_tp):
+            o_arrival(l, lax.rem(tp + j, n_tp), PAIR - 1 - inner).wait_recv()
+
     def ag_far(c):
         r = chunk_rows(c)
         return remote(xf.at[tp, r, :], xf.at[tp, r, :], ag_send.at[0, c], ag_recv.at[0, c], sp, far)
@@ -162,6 +262,18 @@
     def ag_forward(c):
         r = chunk_rows(c)
         return remote(xf.at[far, r, :], xf.at[far, r, :], ag_send.at[2, c], ag_recv.at[2, c], sp, partner)
+
+    def nr_far(c):
+        r = chunk_rows(c)
+        return remote(nrm.at[tp, r, :], nrm.at[tp, r, :], nr_send.at[0, c], nr_recv.at[0, c], sp, far)
+
+    def nr_partner(c):
+        r = chunk_rows(c)
+        return remote(nrm.at[tp, r, :], nrm.at[tp, r, :], nr_send.at[1, c], nr_recv.at[1, c], sp, partner)
+
+    def nr_forward(c):
+        r = chunk_rows(c)
+        return remote(nrm.at[far, r, :], nrm.at[far, r, :], nr_send.at[2, c], nr_recv.at[2, c], sp, partner)
 
     def stat_copy(l, c, step):
         to = lax.rem(tp + step, n_tp)
@@ -171,31 +283,13 @@
         src = lax.rem(tp + step, n_tp)
         return remote(stat.at[l, c, src], stat.at[l, c, src], st_send.at[c, step], st_recv.at[c, src], sp, src)
 
-    def ps_copy(c):
-        r = chunk_rows(c)
-        return remote(ps_out.at[:, r, :], ps_in.at[:, r, :], ps_s.at[c], ps_r.at[c], sp, partner)
-
-    def fs_copy(c):
-        r = chunk_rows(c)
-        return remote(fs_out.at[r, :], fs_in.at[r, :], fs_s.at[c], fs_r.at[c], sp, far)
-
     def rim_copy(l):
         to = lax.rem(sp + 1, n_sp)
         return remote(rim_out.at[l], rim_in.at[l], rim_s.at[l], rim_r.at[l], to, tp)
 
-    for c in range(n_chunks):
-        ag_far(c).start()
-        ag_partner(c).start()
-    for q in range(Z_AHEAD):
-        z_send_all(q % 3, q // 3)
-    for q in range(X_AHEAD):
-        x_own(q % 3, q // 3).start()
-    for p in range(FIRST):
-        q, j = divmod(p, last)
-        if j == 0:
-            z_send_all((q + Z_AHEAD) % 3, (q + Z_AHEAD) // 3)
-            x_own((q + X_AHEAD) % 3, (q + X_AHEAD) // 3).start()
-        relay_piece(q % 3, q // 3, j)
+    def do_pass(c):
+        ag_far(c).wait_recv()
+        ag_forward(c).start()
 
     def do_glu(l, c):
         ag_partner(c).wait_recv()
@@ -248,7 +342,7 @@
         for step in range(1, n_tp):
             stat_copy(l, c, step).start()
 
-    def do_out(l, c):
+    def do_norm(l, c):
         for step in range(1, n_tp):
             stat_arrival(l, c, step).wait_recv()
         r = chunk_rows(c)
@@ -259,130 +353,173 @@
         mean = tot[:, 0:1] / channels
         var = tot[:, 1:2] / channels - mean * mean
         pre = (filt[r, :] - mean) * lax.rsqrt(var + eps) * lng_ref[pl.ds(l, 1), :] + lnb_ref[pl.ds(l, 1), :]
-        normed = jax.nn.silu(pre).astype(jnp.bfloat16)
-        for step in range(1, n_tp):
-            stat_copy(l, c, step).wait_send()
+        nrm[tp, r, :] = jax.nn.silu(pre).astype(jnp.bfloat16)
         ag_far(c).wait_send()
         ag_partner(c).wait_send()
         ag_forward(c).wait_send()
-        for half in range(n_tp // PAIR):
-            for q in range(per_blk):
-                cols = slice(q * width, (q + 1) * width)
-                away = (half * PAIR + (PAIR - 1 - core)) * per_blk + q
-                ps_out[half, r, cols] = jnp.dot(
-                    normed, wo_all[l, away], preferred_element_type=jnp.float32).astype(jnp.bfloat16)
-        ps_copy(c).start()
-        for half in range(n_tp // PAIR):
-            for q in range(per_blk):
-                cols = slice(q * width, (q + 1) * width)
-                mine = (half * PAIR + core) * per_blk + q
-                keep[half, r, cols] = jnp.dot(normed, wo_all[l, mine], preferred_element_type=jnp.float32)
-
-    def do_pair(l, c):
-        ps_copy(c).wait_recv()
-        r = chunk_rows(c)
-        other = n_tp // PAIR - 1 - far_half
-        fs_out[r, :] = (keep[other, r, :] + ps_in[other, r, :].astype(jnp.float32)).astype(jnp.bfloat16)
-        fs_copy(c).start()
-
-    def do_final(l, c):
-        fs_copy(c).wait_recv()
-        ps_copy(c).wait_send()
-        fs_copy(c).wait_send()
-        r = chunk_rows(c)
-        branch = keep[far_half, r, :] + ps_in[far_half, r, :].astype(jnp.float32) + fs_in[r, :].astype(jnp.float32)
-        new = (xf[tp, r, :].astype(jnp.float32) + branch).astype(jnp.bfloat16)
+        for step in range(1, n_tp):
+            stat_copy(l, c, step).wait_send()
+        nr_far(c).start()
+        nr_partner(c).start()
+
+    def do_hand(c):
+        nr_far(c).wait_recv()
+        nr_forward(c).start()
+
+    def do_out(l, c):
+        nr_partner(c).wait_recv()
+        nr_forward(c).wait_recv()
+        r = chunk_rows(c)
+        full = jnp.concatenate([nrm[b, r, :] for b in range(n_tp)], axis=1)
+        for q in range(PAIR):
+            cols = slice(q * width, (q + 1) * width)
+            branch = jnp.dot(full, wo_all[l, q], preferred_element_type=jnp.float32)
+            out_ref[r, cols] = (xf[tp, r, cols].astype(jnp.float32) + branch).astype(jnp.bfloat16)
+
+        nr_far(c).wait_send()
+        nr_partner(c).wait_send()
+        nr_forward(c).wait_send()
 
         @pl.when(l < layers - 1)
         def _():
-            xf[tp, r, :] = new
+            xf[tp, r, :] = out_ref[r, :]
             ag_far(c).start()
             ag_partner(c).start()
 
-        @pl.when(l == layers - 1)
-        def _():
-            out_ref[r, :] = new
+    by_head = near_end * (outer - tp) * (outer - tp) * (1 - (far_half - core) * (far_half - core)) == 1
+    is_mid = (near_end == 1) & jnp.logical_not(by_head)
+    is_head = (near_end == 0) & (outer == tp)
+    is_end = (near_end == 0) & (outer != tp)
+
+    roles = (
+        (is_end, END_OPEN, END_PLAN), (is_head, HEAD_OPEN, HEAD_PLAN),
+        (is_mid, MID_OPEN, MID_PLAN), (by_head, NEXT_OPEN, NEXT_PLAN),
+    )
+
+    def act(kind, j, l, side):
+        if kind == ZOWN:
+            z_own(j, l)
+        elif kind == XOWN:
+            x_own(j, l).start()
+        elif kind >= O:
+            relay_o(l, j, kind)
+        else:
+            relay_piece(kind, l, j, side and kind == G)
+
+    for m in (V, G):
+        z_own(m, 0)
+        x_own(m, 0).start()
+    send_o(0)
+    for c in range(n_chunks):
+        ag_far(c).start()
+        ag_partner(c).start()
+    for role, order, _ in roles:
+        @pl.when(role)
+        def _():
+            for kind, j, later in order:
+                act(kind, j, later, False)
+
+    for c in range(n_chunks):
+        do_pass(c)
+    w_ready(V, 0)
+    w_ready(G, 0)
 
     def layer_body(l, carry):
-        base = lax.rem(l, n_chunks)
         more = l < layers - 1
 
-        def step_body(i, inner_carry):
-            def at(back):
-                return lax.rem(base + i + n_chunks * 2 - back, n_chunks)
-
-            for k in range(3 * last):
-                q, j = divmod(FIRST + k, last)
-                if j == 0:
-                    z_next, x_next = q + Z_AHEAD, q + X_AHEAD
-
-                    @pl.when((i == STEPS[k]) & (l + z_next // 3 < layers))
+        def at(k):
+            return lax.rem(l + k, n_chunks)
+
+        def ahead(f):
+            pl.when(more)(f)
+
+        def slot(n):
+            for role, _, plan in roles:
+                for kind, j, later in plan.get(n, ()):
+                    @pl.when((role & (l + later < layers)) if later else role)
                     def _():
-                        z_send_all(z_next % 3, l + z_next // 3)
-
-                    @pl.when((i == STEPS[k]) & (l + x_next // 3 < layers))
-                    def _():
-                        x_own(x_next % 3, l + x_next // 3).start()
-
-                @pl.when((i == STEPS[k]) & (l + q // 3 < layers))
-                def _():
-                    relay_piece(q % 3, l + q // 3, j)
-
-            @pl.when(i < n_chunks)
-            def _():
-                ag_far(at(0)).wait_recv()
-                ag_forward(at(0)).start()
-
-            @pl.when(i == 0)
-            def _():
-                w_ready(0, l)
-                w_ready(1, l)
-
-            @pl.when((i >= 2) & (i < n_chunks + 2))
-            def _():
-                do_conv(l, at(1))
-
-            @pl.when(i < n_chunks)
-            def _():
-                do_glu(l, at(0))
-
-            @pl.when(i == 3)
-            def _():
-                w_ready(2, l)
-
-            @pl.when((i >= 3) & (i < n_chunks + 3))
-            def _():
-                do_out(l, at(2))
-
-            @pl.when((i >= 4) & (i < n_chunks + 4))
-            def _():
-                do_pair(l, at(3))
-
-            @pl.when(i >= 5)
-            def _():
-                do_final(l, at(4))
-
-            return inner_carry
-
-        lax.fori_loop(0, n_chunks + 5, step_body, 0)
+                        act(kind, j, l + later, True)
+
+        def pass_next(k):
+            ahead(lambda: do_pass(at(k + 1)))
+
+        do_glu(l, at(0))
+        do_glu(l, at(1))
+        do_conv(l, at(1))
+        ahead(lambda: send_o(l + 1))
+        slot(1)
+        do_glu(l, at(2))
+        do_conv(l, at(2))
+        do_glu(l, at(3))
+        slot(2)
+        do_conv(l, at(3))
+        do_norm(l, at(1))
+        do_conv(l, at(0))
+        do_norm(l, at(2))
+        do_norm(l, at(3))
+        slot(3)
+        do_norm(l, at(0))
+        slot(4)
+        do_hand(at(1))
+        do_hand(at(2))
+        slot(5)
+        do_hand(at(3))
+        do_hand(at(0))
+        slot(6)
+        o_ready(l)
+        do_out(l, at(1))
+        do_out(l, at(2))
+        slot(7)
+        do_out(l, at(3))
+        do_out(l, at(0))
+
+        slot(8)
+        pass_next(0)
+        slot(9)
+        pass_next(1)
+        slot(10)
+        pass_next(2)
+        slot(11)
+        pass_next(3)
+        slot(12)
+
+        @pl.when(more)
+        def _():
+            w_ready(V, l + 1)
+            w_ready(G, l + 1)
 
         return carry
 
     lax.fori_loop(0, layers, layer_body, 0)
 
     def drain(l, carry):
-        for m in range(3):
-            for j in range(last - 1):
-                z_copy(m, l, j).wait_send()
+        for m in range(PAIR):
+            z_copy(m, l, 0).wait_send()
 
             @pl.when(near_end == 1)
             def _():
-                z_copy(m, l, last - 1).wait_send()
-                z_forward(m, l).wait_send()
+                z_copy(m, l, 1).wait_send()
+                for j in range(last):
+                    z_forward(m, l, j).wait_send()
 
             for j in range(last):
-                (side_copy(m, l) if j == 0 and m in SIDE else x_copy(m, l, j)).wait_send()
+                x_copy(m, l, j).wait_send()
             x_own(m, l).wait_send()
+
+        @pl.when(outer != tp)
+        def _():
+            o_gather(l).wait_send()
+
+        for j in range(n_tp):
+            @pl.when(goes_up)
+            def _():
+                o_hop(l, j, 0, sp + PAIR).wait_send()
+
+            @pl.when(goes_down)
+            def _():
+                o_hop(l, j, 1, sp - PAIR).wait_send()
+
+            o_hop(l, j, 2, x_peer).wait_send()
 
         @pl.when(sp < n_sp - 1)
         def _():
@@ -399,7 +536,6 @@
     width = w_out.shape[2]
     n_chunks = rows // CHUNK
     features = dblk * n_tp
-    n_half = n_tp // PAIR
     bf16, f32 = jnp.bfloat16, jnp.float32
     dma = pltpu.SemaphoreType.DMA
     vmem = pl.BlockSpec(memory_space=pltpu.VMEM)
@@ -411,7 +547,7 @@
         scratch_shapes=[
             pltpu.VMEM((layers, n_sp * depth, chan), bf16),
             pltpu.VMEM((layers, n_sp * depth, chan), bf16),
-            pltpu.VMEM((layers, n_sp, chan, width), bf16),
+            pltpu.VMEM((layers, PAIR, n_tp * chan, width), bf16),
             pltpu.VMEM((n_tp, rows, dblk), bf16),
             pltpu.VMEM((CHUNK, features), bf16),
             pltpu.VMEM((chan // LANES, HALO + rows, LANES), f32),
@@ -419,24 +555,21 @@
             pltpu.VMEM((layers, HALO, chan), bf16),
             pltpu.VMEM((layers, HALO, chan), bf16),
             pltpu.VMEM((layers, n_chunks, n_tp, 8, CHUNK), f32),
-            pltpu.VMEM((n_half, rows, dblk), bf16),
-            pltpu.VMEM((n_half, rows, dblk), bf16),
-            pltpu.VMEM((n_half, rows, dblk), f32),
-            pltpu.VMEM((rows, dblk), bf16),
-            pltpu.VMEM((rows, dblk), bf16),
-            dma((layers, 3, n_sp)),
-            dma((layers, 3, n_sp // PAIR)),
-            dma((layers, 3, n_sp // PAIR)),
+            pltpu.VMEM((n_tp, rows, chan), bf16),
+            dma((layers, PAIR, n_sp)),
+            dma((layers, PAIR, n_sp // PAIR + 1)),
+            dma((layers, PAIR, n_sp // PAIR)),
+            dma((layers, n_tp, PAIR)),
+            dma((layers, n_tp, 3)),
+            dma((layers,)),
             dma((3, n_chunks)),
             dma((3, n_chunks)),
             dma((layers,)),
             dma((layers,)),
             dma((n_chunks, n_tp)),
             dma((n_chunks, n_tp)),
-            dma((n_chunks,)),
-            dma((n_chunks,)),
-            dma((n_chunks,)),
-            dma((n_chunks,)),
+            dma((3, n_chunks)),
+            dma((3, n_chunks)),
         ],
         compiler_params=pltpu.CompilerParams(collective_id=0, has_side_effects=True),
     )(
@@ -463,7 +596,7 @@
         and w_value.shape[1] % LANES == 0
         and w_value.shape[2] % LANES == 0
         and width % LANES == 0
-        and dblk % width == 0
+        and dblk == PAIR * width
         and conv_taps.shape[1] - 1 <= HALO
     )
 

time: 137 us -> 127 us (0.927); the launches traced: 134 us -> 127 us
  Pallas kernels: 133 us -> 125 us
    pallas_call x1, Pallas kernels: 133 us -> 125 us  [fused_shards(): pl.pallas_call(functools.partial(fused_kernel, n_sp, n_tp, 1e-06), out_sh...]
where the time goes in v1:
time: 127 us
  Pallas kernels  125 us (98%)
  local copies, waits for them, and re-layouts  1.87 us (1%)
    pallas_call x1, Pallas kernels, fused_shards(): pl.pallas_call(functools.partial(fused_kernel, n_sp, n_tp, 1e-06), out_sh...  125 us

profile of v1, /device:TPU:3, one launch (start us, length us, event | category | flops | bytes accessed | tf_op | source)
XLA Modules:
  0.0 127.0 jit_solution(4834274897636088142)
XLA Ops:
  0.0 125.1 %shard_map.82 = bf16[512,512]{1,0:T(8,128)(2,1)} custom-call(bf16[512,512]{1,0:T(8,128)(2,1)} %x_ref.1, f32[3,2048]{1,0:T(4,128)} %gain_ref.1, bf16[3,256,256]{2,1,0:T(8,128)(2,1)} %wv_ref.1, bf16[3,256,256]{2,1,0:T(8,128)(2,1)} %wg_ref.1, f32[3,31,256]{2,1,0:T(8,128)} %taps_ref.1, f32[3,256]{1,0:T(4,128)} %lng_ref.1, f32[3,256]{1,0:T(4,128)} %lnb_ref.1, ...), custom_call_target="tpu_custom_call" | custom-call | tf_op jit(solution)/shard_map/pallas_call | solution.py:542
  125.2 1.9 %copy.10 = bf16[512,512]{1,0:T(8,128)(2,1)} copy(bf16[512,512]{1,0:T(8,128)(2,1)} %shard_map.82) | data formatting | bytes 1048576

commit v2 on v1

v2 whole, which is shorter than its diff:
```python
import functools

import jax
import jax.numpy as jnp
from jax import lax
from jax.experimental import pallas as pl
from jax.experimental.pallas import tpu as pltpu
from jax.sharding import PartitionSpec as P

MESH = pl.DeviceIdType.MESH
PAIR = 2
CHUNK = 128
HALO = 32
LANES = 128
V, G, O, UP, OVER, ZOWN, XOWN, BEFORE, SIDE = 0, 1, 2, 3, 4, 5, 6, 7, 8
OWN_X = ((XOWN, V, 1), (XOWN, G, 1))
OWN_Z = ((ZOWN, V, 1), (ZOWN, G, 1))
RISEN, FIRST = -1, -2
LAST_X = ((XOWN, V, 2), (XOWN, G, 2))
LAST_Z = ((ZOWN, V, 2), (ZOWN, G, 2))


def every(kind, later):
    return tuple((kind, j, later) for j in range(4))


END_OPEN = (
    (V, 0, 0), *OWN_Z, (G, 0, 0), (V, 1, 0), (BEFORE, 0, 0), (G, 1, 0), (V, 2, 0), (G, 2, 0), (O, 0, 0),
    (XOWN, V, 1),
)
HEAD_OPEN = (
    (V, 0, 0), *every(UP, 0), *OWN_Z, (G, 0, 0), (V, 1, 0), (BEFORE, 0, 0), (G, 1, 0), (V, 2, 0), (G, 2, 0),
    *every(OVER, 0), *OWN_X,
)
MID_OPEN = (
    (V, 0, 0), (V, 1, 0), (G, 0, 0), (G, 1, 0), (V, 2, 0), (BEFORE, 0, 0), (G, 2, 0),
    (O, 0, 0), (O, 1, 0), (ZOWN, V, 1), (O, 2, 0),
)
NEAR_OPEN = (
    (V, 0, 0), (V, 1, 0), (G, 0, 0), (G, 1, 0), (V, 2, 0), (BEFORE, 0, 0), (G, 2, 0),
    *every(O, 0), *OWN_Z, *OWN_X,
)
END_PLAN = {
    1: ((O, 0, RISEN), (O, 1, 0)), 2: ((O, 2, 0), (XOWN, G, 1)), 3: ((O, 3, 0),), 5: ((V, 0, 1), *LAST_Z),
    6: ((V, 1, 1),), 7: ((V, 2, 1),), 8: ((G, 0, 1), (SIDE, 0, 1)), 9: ((G, 1, 1),), 10: ((G, 2, 1),),
    12: ((XOWN, V, 2),),
}
HEAD_PLAN = {
    3: every(UP, 1), 5: ((V, 0, 1), *LAST_Z), 6: ((V, 1, 1),), 7: ((V, 2, 1),),
    8: ((G, 0, 1), (SIDE, 0, 1)), 9: ((G, 1, 1),), 10: ((G, 2, 1), *every(OVER, 1), *LAST_X),
}
MID_PLAN = {
    1: ((O, 3, FIRST), (ZOWN, G, 1), *OWN_X), 3: ((V, 0, 1),), 4: ((V, 1, 1), (V, 2, 1)),
    5: ((G, 0, 1),), 6: ((G, 1, 1),), 7: ((G, 2, 1), (SIDE, 0, 1)),
    9: ((O, 0, 1),), 10: ((O, 1, 1),), 11: ((O, 2, 1),), 12: ((O, 3, 1), (ZOWN, V, 2)),
}
ROOT_PLAN = {
    1: ((V, 0, 1),), 2: ((V, 1, 1),), 3: ((V, 2, 1),), 4: ((G, 0, 1),), 5: ((G, 1, 1),),
    6: ((G, 2, 1),), 7: ((SIDE, 0, 1), (O, 0, 1), (O, 1, 1)), 8: ((O, 2, 1), (O, 3, 1), *LAST_Z, *LAST_X),
}
NEXT_PLAN = {
    1: ((V, 0, 1),), 2: ((V, 1, 1),), 3: ((V, 2, 1),), 4: ((G, 0, 1), (UP, 0, 1)), 5: ((G, 1, 1), (UP, 1, 1)),
    6: ((G, 2, 1), (UP, 2, 1)), 7: ((SIDE, 0, 1), (UP, 3, 1)),
    8: (*every(OVER, 1), *LAST_Z, *LAST_X),
}


def fused_kernel(
    n_sp, n_tp, eps,
    x_ref, gain_hbm, wv_ref, wg_ref, taps_hbm, lng_hbm, lnb_hbm, wo_ref,
    out_ref,
    gain_ref, taps_ref, lng_ref, lnb_ref, out_all, wv_all, wg_all, wo_all, xf, hid, glu, filt, stat, nrm,
    w_recv, w_zsend, w_xsend, o_recv, o_send, og_send,
    ag_recv, ag_send, before_s, before_r, st_recv, st_send, nr_recv, nr_send,
    in_sem, small_sem, out_sem,
):
    sp = lax.axis_index("sp")
    tp = lax.axis_index("tp")
    layers, depth = wv_ref.shape[0], wv_ref.shape[1]
    rows, dblk = x_ref.shape
    width = wo_ref.shape[2]
    chan = wv_ref.shape[2]
    taps = taps_ref.shape[1]
    features = dblk * n_tp
    channels = chan * n_tp
    n_chunks = rows // CHUNK
    n_out = n_sp // PAIR
    outer, inner = lax.div(sp, PAIR), lax.rem(sp, PAIR)
    x_peer = outer * PAIR + (PAIR - 1 - inner)
    far_half, core = lax.div(tp, PAIR), lax.rem(tp, PAIR)
    partner = far_half * PAIR + (PAIR - 1 - core)
    far = (n_tp // PAIR - 1 - far_half) * PAIR + core
    first_off = HALO - (taps - 1)
    ext = HALO * layers
    halves = chan // LANES

    last = n_out - 1
    upper = lax.div(outer, n_out // 2)
    near_end = outer + upper * (last - 2 * outer)

    def line(j):
        near = j + 1 - (near_end if j == 0 else 0)
        return near + upper * (last - 2 * near)

    slant = sp + 2 * inner - 1
    has_slant = (slant >= 0) & (slant < n_sp)
    barrier = pltpu.get_barrier_semaphore()

    def greet(sp_to, tp_to):
        pl.semaphore_signal(barrier, inc=1, device_id=(sp_to, tp_to), device_id_type=MESH)

    greet(line(0) * PAIR + inner, tp)
    greet(x_peer, tp)
    for step in range(1, n_tp):
        greet(sp, lax.rem(tp + step, n_tp))

    @pl.when(near_end == 1)
    def _():
        greet(line(1) * PAIR + inner, tp)

    @pl.when(has_slant)
    def _():
        greet(slant, tp)

    def own_rows(s):
        return pl.ds(pl.multiple_of(s * depth, depth), depth)

    def o_slot(l, x, b):
        return wo_all.at[l, x, pl.ds(pl.multiple_of(b * chan, chan), chan), :]

    def load_weight(m, l):
        src, dst = ((wv_ref, wv_all), (wg_ref, wg_all))[m]
        return pltpu.make_async_copy(src.at[l], dst.at[l, own_rows(sp), :], in_sem.at[m, l])

    def load_out(l):
        return pltpu.make_async_copy(wo_ref.at[l], o_slot(l, inner, tp), in_sem.at[2, l])

    def load_rows():
        return pltpu.make_async_copy(x_ref, xf.at[tp, pl.ds(ext, rows), :], small_sem.at[4])

    smalls = [
        pltpu.make_async_copy(src, dst, small_sem.at[i])
        for i, (src, dst) in enumerate(
            ((gain_hbm, gain_ref), (taps_hbm, taps_ref), (lng_hbm, lng_ref), (lnb_hbm, lnb_ref)))
    ]
    for m in range(PAIR):
        load_weight(m, 0).start()
    load_rows().start()

    @pl.when(outer == tp)
    def _():
        for l in range(layers):
            load_out(l).start()

    for l in range(1, layers):
        for m in range(PAIR):
            load_weight(m, l).start()
    for small in smalls:
        small.start()

    glu[:, 0:HALO, :] = jnp.zeros((halves, HALO, LANES), jnp.float32)

    @pl.when(sp == 0)
    def _():
        xf[tp, 0:ext, :] = jnp.zeros((ext, dblk), jnp.bfloat16)


    for m in range(PAIR):
        load_weight(m, 0).wait()
    pl.semaphore_wait(barrier, 2 + n_tp - 1 + near_end + has_slant.astype(jnp.int32))

    def parts(c):
        own = (ext + c * CHUNK, CHUNK)
        return ((0, ext), own) if c == 0 else (own,)

    def chunk_rows(c, skip):
        return pl.ds(ext + c * CHUNK, CHUNK) if c else pl.ds(skip * HALO, ext - skip * HALO + CHUNK)

    def by_layer(c, l, f):
        if c or isinstance(l, int):
            f(0 if c else l)
        else:
            for k in range(layers):
                pl.when(l == k)(functools.partial(f, k))

    def stat_rows(c):
        return pl.ds(0, 8 * len(parts(c)))

    def remote(src, dst, send, recv, sp_to, tp_to):
        return pltpu.make_async_remote_copy(
            src_ref=src, dst_ref=dst, send_sem=send, recv_sem=recv,
            device_id=(sp_to, tp_to), device_id_type=MESH,
        )

    def w_slot(m, l, s):
        return (wv_all, wg_all)[m].at[l, own_rows(s), :]

    def z_copy(m, l, j):
        to = line(j) * PAIR + inner
        return remote(w_slot(m, l, sp), w_slot(m, l, sp), w_zsend.at[l, m, j], w_recv.at[l, m, sp], to, tp)

    def z_arrival(m, l, j):
        s = line(j) * PAIR + inner
        return remote(w_slot(m, l, s), w_slot(m, l, s), w_zsend.at[l, m, j], w_recv.at[l, m, s], s, tp)

    def z_forward(m, l, j):
        s = line(j) * PAIR + inner
        to = line(1 if j == 0 else 0) * PAIR + inner
        slot = w_slot(m, l, s)
        return remote(slot, slot, w_zsend.at[l, m, PAIR + j], w_recv.at[l, m, s], to, tp)

    def x_own(m, l):
        return remote(w_slot(m, l, sp), w_slot(m, l, sp), w_xsend.at[l, m, last], w_recv.at[l, m, sp], x_peer, tp)

    def x_copy(m, l, j):
        s = line(j) * PAIR + inner
        slot = w_slot(m, l, s)
        return remote(slot, slot, w_xsend.at[l, m, j], w_recv.at[l, m, s], x_peer, tp)

    def x_arrival(m, l, z):
        s = z * PAIR + (PAIR - 1 - inner)
        slot = w_slot(m, l, s)
        return remote(slot, slot, w_xsend.at[l, m, last], w_recv.at[l, m, s], x_peer, tp)

    def side_copy(m, l):
        to = line(0) * PAIR + inner
        slot = w_slot(m, l, x_peer)
        return remote(slot, slot, w_xsend.at[l, m, 0], w_recv.at[l, m, x_peer], to, tp)

    def z_own(m, l):
        z_copy(m, l, 0).start()

        @pl.when(near_end == 1)
        def _():
            z_copy(m, l, 1).start()

    def relay_piece(m, l, j, side):
        z_arrival(m, l, j).wait_recv()

        @pl.when(near_end == 1)
        def _():
            z_forward(m, l, j).start()

        if j or not side:
            x_copy(m, l, j).start()

    def relay_side(m, l):
        x_arrival(m, l, outer).wait_recv()
        side_copy(m, l).start()

    def w_ready(m, l):
        if m == 1:
            @pl.when(l == 0)
            def _():
                x_arrival(m, l, outer).wait_recv()
        else:
            x_arrival(m, l, outer).wait_recv()
        for j in range(last):
            x_arrival(m, l, line(j)).wait_recv()

    def o_gather(l):
        return remote(wo_ref.at[l], o_slot(l, inner, tp), og_send.at[l], o_recv.at[l, tp, inner], sp, outer)

    def o_hop(l, j, way, to):
        b = lax.rem(tp + j, n_tp)
        slot = o_slot(l, inner, b)
        return remote(slot, slot, o_send.at[l, j, way], o_recv.at[l, b, inner], to, tp)

    def o_arrival(l, b, x):
        slot = o_slot(l, x, b)
        return remote(slot, slot, o_send.at[l, 0, 0], o_recv.at[l, b, x], x_peer, tp)

    goes_up = (outer >= tp) & (outer < last)
    goes_down = (outer <= tp) & (outer > 0)

    def send_o(l):
        @pl.when(outer != tp)
        def _():
            o_gather(l).start()

    def o_arrived(l, j):
        if j == 0:
            @pl.when(outer != tp)
            def _():
                o_arrival(l, tp, inner).wait_recv()
        else:
            o_arrival(l, lax.rem(tp + j, n_tp), inner).wait_recv()

    def o_along(l, j):
        @pl.when(goes_up)
        def _():
            o_hop(l, j, 0, sp + PAIR).start()

        @pl.when(goes_down)
        def _():
            o_hop(l, j, 1, sp - PAIR).start()

    def relay_o(l, j, kind):
        if kind != OVER:
            o_arrived(l, j)
            o_along(l, j)
        if kind != UP:
            o_hop(l, j, 2, x_peer).start()

    def o_ready(l):
        for j in range(n_tp):
            o_arrival(l, lax.rem(tp + j, n_tp), PAIR - 1 - inner).wait_recv()

    def ag_far(c, l):
        r = chunk_rows(c, l)
        return remote(xf.at[tp, r, :], xf.at[tp, r, :], ag_send.at[0, c], ag_recv.at[0, c], sp, far)

    def ag_partner(c, l):
        r = chunk_rows(c, l)
        return remote(xf.at[tp, r, :], xf.at[tp, r, :], ag_send.at[1, c], ag_recv.at[1, c], sp, partner)

    def ag_forward(c, l):
        r = chunk_rows(c, l)
        return remote(xf.at[far, r, :], xf.at[far, r, :], ag_send.at[2, c], ag_recv.at[2, c], sp, partner)

    def nr_far(c, l):
        r = chunk_rows(c, l + 1)
        return remote(nrm.at[tp, r, :], nrm.at[tp, r, :], nr_send.at[0, c], nr_recv.at[0, c], sp, far)

    def nr_partner(c, l):
        r = chunk_rows(c, l + 1)
        return remote(nrm.at[tp, r, :], nrm.at[tp, r, :], nr_send.at[1, c], nr_recv.at[1, c], sp, partner)

    def nr_forward(c, l):
        r = chunk_rows(c, l + 1)
        return remote(nrm.at[far, r, :], nrm.at[far, r, :], nr_send.at[2, c], nr_recv.at[2, c], sp, partner)

    def stat_copy(l, c, step):
        to = lax.rem(tp + step, n_tp)
        return remote(stat.at[l, c, tp, stat_rows(c), :], stat.at[l, c, tp, stat_rows(c), :], st_send.at[c, step], st_recv.at[c, tp], sp, to)

    def stat_arrival(l, c, step):
        src = lax.rem(tp + step, n_tp)
        return remote(stat.at[l, c, src, stat_rows(c), :], stat.at[l, c, src, stat_rows(c), :], st_send.at[c, step], st_recv.at[c, src], sp, src)

    def before_copy():
        to = lax.rem(sp + 1, n_sp)
        return remote(x_ref.at[pl.ds(rows - ext, ext), :], xf.at[tp, pl.ds(0, ext), :], before_s.at[0], before_r.at[0], to, tp)

    def do_pass(l, c):
        def go(k):
            ag_far(c, k).wait_recv()
            ag_forward(c, k).start()

        by_layer(c, l, go)

    def ag_start(l, c):
        def go(k):
            ag_far(c, k).start()
            ag_partner(c, k).start()

        by_layer(c, l, go)

    def ag_sent(l, c):
        def go(k):
            ag_far(c, k).wait_send()
            ag_partner(c, k).wait_send()
            ag_forward(c, k).wait_send()

        by_layer(c, l, go)

    def ag_wait(l, c):
        def go(k):
            ag_partner(c, k).wait_recv()
            ag_forward(c, k).wait_recv()

        by_layer(c, l, go)

    def nr_start(l, c):
        def go(k):
            nr_far(c, k).start()
            nr_partner(c, k).start()

        by_layer(c, l, go)

    def nr_sent(l, c):
        def go(k):
            nr_far(c, k).wait_send()
            nr_partner(c, k).wait_send()
            nr_forward(c, k).wait_send()

        by_layer(c, l, go)

    def nr_wait(l, c):
        def go(k):
            nr_partner(c, k).wait_recv()
            nr_forward(c, k).wait_recv()

        by_layer(c, l, go)

    def do_glu(l, c):
        ag_wait(l, c)
        for start, size in parts(c):
            r = slice(start, start + size)
            blocks = [xf[b, r, :].astype(jnp.float32) for b in range(n_tp)]
            total = sum(jnp.sum(b * b, axis=1, keepdims=True) for b in blocks)
            scale = lax.rsqrt(total / features + eps)
            for b in range(n_tp):
                cols = slice(b * dblk, (b + 1) * dblk)
                hid[0:size, cols] = (
                    xf[b, r, :].astype(jnp.float32) * scale * gain_ref[pl.ds(l, 1), cols]).astype(jnp.bfloat16)
            h = hid[0:size, :]
            value = jnp.dot(h, wv_all[l], preferred_element_type=jnp.float32)
            gate = jnp.dot(h, wg_all[l], preferred_element_type=jnp.float32)
            g = (value * jax.nn.sigmoid(gate)).astype(jnp.bfloat16).astype(jnp.float32)
            if start < ext:
                g = jnp.where(sp > 0, g, 0.0)
            for k in range(halves):
                glu[k, HALO + start:HALO + start + size, :] = g[:, k * LANES:(k + 1) * LANES]

    def do_conv(l, c):
        for i, (start, size) in enumerate(parts(c)):
            sums = jnp.zeros((size, 1), jnp.float32)
            squares = jnp.zeros((size, 1), jnp.float32)
            for k in range(halves):
                acc = jnp.zeros((size, LANES), jnp.float32)
                for tap in range(taps):
                    acc = acc + taps_ref[l, tap:tap + 1, k * LANES:(k + 1) * LANES] * glu[
                        k, start + first_off + tap:start + first_off + tap + size, :]
                filt[start:start + size, k * LANES:(k + 1) * LANES] = acc
                sums = sums + jnp.sum(acc, axis=1, keepdims=True)
                squares = squares + jnp.sum(acc * acc, axis=1, keepdims=True)
            lane = lax.broadcasted_iota(jnp.int32, (size, LANES), 1)
            both = jnp.where(lane == 0, sums, squares)
            if size < CHUNK:
                both = jnp.concatenate([both, jnp.zeros((CHUNK - size, LANES), jnp.float32)], axis=0)
            stat[l, c, tp, 8 * i:8 * i + 8, :] = jnp.transpose(both)[0:8, :]
        for step in range(1, n_tp):
            stat_copy(l, c, step).start()

    def do_norm(l, c):
        for step in range(1, n_tp):
            stat_arrival(l, c, step).wait_recv()
        def norm_part(i, start, size):
            r = slice(start, start + size)
            tot = stat[l, c, 0, 8 * i:8 * i + 8, :]
            for b in range(1, n_tp):
                tot = tot + stat[l, c, b, 8 * i:8 * i + 8, :]
            tot = jnp.transpose(jnp.concatenate([tot, jnp.zeros((LANES - 8, CHUNK), jnp.float32)], axis=0))
            mean = tot[0:size, 0:1] / channels
            var = tot[0:size, 1:2] / channels - mean * mean
            pre = (filt[r, :] - mean) * lax.rsqrt(var + eps) * lng_ref[pl.ds(l, 1), :] + lnb_ref[pl.ds(l, 1), :]
            nrm[tp, r, :] = jax.nn.silu(pre).astype(jnp.bfloat16)

        for i, (start, size) in enumerate(parts(c)):
            pl.when((start >= ext) | (l < layers - 1))(functools.partial(norm_part, i, start, size))
        ag_sent(l, c)
        for step in range(1, n_tp):
            stat_copy(l, c, step).wait_send()
        nr_start(l, c)

    def do_hand(l, c):
        def go(k):
            nr_far(c, k).wait_recv()
            nr_forward(c, k).start()

        by_layer(c, l, go)

    def store_rows(c):
        r = pl.ds(c * CHUNK, CHUNK)
        return pltpu.make_async_copy(out_all.at[r, :], out_ref.at[r, :], out_sem.at[c])

    def do_out(l, c):
        nr_wait(l, c)
        def out_part(start, size):
            r = slice(start, start + size)
            full = jnp.concatenate([nrm[b, r, :] for b in range(n_tp)], axis=1)
            for q in range(PAIR):
                cols = slice(q * width, (q + 1) * width)
                branch = jnp.dot(full, wo_all[l, q], preferred_element_type=jnp.float32)
                new = (xf[tp, r, cols].astype(jnp.float32) + branch).astype(jnp.bfloat16)
                xf[tp, r, cols] = new
                if start >= ext:
                    out_all[start - ext:start - ext + size, cols] = new

        for start, size in parts(c):
            pl.when((start >= ext) | (l < layers - 1))(functools.partial(out_part, start, size))

        @pl.when(l < layers - 1)
        def _():
            ag_start(l + 1, c)

        @pl.when(l == layers - 1)
        def _():
            store_rows(c).start()

        nr_sent(l, c)

    by_head = near_end * (outer - tp) * (outer - tp) * (1 - (far_half - core) * (far_half - core)) == 1
    is_root = (near_end == 1) & (outer == tp)
    is_mid = (near_end == 1) & (outer != tp) & jnp.logical_not(by_head)
    is_head = (near_end == 0) & (outer == tp)
    is_end = (near_end == 0) & (outer != tp)

    roles = (
        (is_end, END_OPEN, END_PLAN), (is_head, HEAD_OPEN, HEAD_PLAN),
        (is_mid, MID_OPEN, MID_PLAN), (is_root, NEAR_OPEN, ROOT_PLAN), (by_head, NEAR_OPEN, NEXT_PLAN),
    )

    def act(kind, j, l, side):
        if kind == BEFORE:
            @pl.when(sp > 0)
            def _():
                before_copy().wait_recv()

            ag_start(0, 0)
        elif kind == SIDE:
            relay_side(G, l)
        elif kind == ZOWN:
            z_own(j, l)
        elif kind == XOWN:
            x_own(j, l).start()
        elif kind >= O:
            relay_o(l, j, kind)
        else:
            relay_piece(kind, l, j, side and kind == G)

    for m in (V, G):
        z_own(m, 0)
        x_own(m, 0).start()
    @pl.when(sp < n_sp - 1)
    def _():
        before_copy().start()

    send_o(0)
    load_rows().wait()
    for c in range(1, n_chunks):
        ag_start(0, c)
    for l in range(1, layers):
        for m in range(PAIR):
            load_weight(m, l).wait()

    @pl.when(outer == tp)
    def _():
        for l in range(layers):
            load_out(l).wait()

    for small in smalls:
        small.wait()
    for role, order, _ in roles:
        @pl.when(role)
        def _():
            for kind, j, later in order:
                act(kind, j, later, False)

    for c in range(n_chunks):
        do_pass(0, c)
    w_ready(V, 0)
    w_ready(G, 0)

    def layer_body(l, carry):
        more = l < layers - 1

        def ahead(f):
            pl.when(more)(f)

        def slot(n):
            for role, _, plan in roles:
                for kind, j, later in plan.get(n, ()):
                    if later == RISEN:
                        when = role & (l > 0)
                    elif later == FIRST:
                        when = role & (l == 0)
                    else:
                        when = (role & (l + later < layers)) if later else role

                    @pl.when(when)
                    def _():
                        act(kind, j, l + max(later, 0), True)

        def pass_next(c):
            ahead(lambda: do_pass(l + 1, c))

        do_glu(l, 0)
        do_conv(l, 0)
        ahead(lambda: send_o(l + 1))
        slot(1)
        do_glu(l, 1)
        do_conv(l, 1)
        do_glu(l, 2)
        do_conv(l, 2)
        slot(2)
        do_norm(l, 0)
        do_glu(l, 3)
        do_conv(l, 3)
        do_norm(l, 1)
        slot(3)
        do_norm(l, 2)
        do_norm(l, 3)
        slot(4)
        do_hand(l, 0)
        slot(5)
        do_hand(l, 1)
        o_ready(l)
        do_out(l, 0)
        do_hand(l, 2)
        do_out(l, 1)
        slot(6)
        do_hand(l, 3)
        do_out(l, 2)
        slot(7)
        do_out(l, 3)
        slot(8)
        pass_next(0)
        slot(9)
        pass_next(1)
        slot(10)
        pass_next(2)
        slot(11)
        pass_next(3)
        slot(12)

        @pl.when(more)
        def _():
            w_ready(V, l + 1)
            w_ready(G, l + 1)

        return carry

    lax.fori_loop(0, layers, layer_body, 0)

    def drain(l, carry):
        for m in range(PAIR):
            z_copy(m, l, 0).wait_send()

            @pl.when(near_end == 1)
            def _():
                z_copy(m, l, 1).wait_send()
                for j in range(last):
                    z_forward(m, l, j).wait_send()

            for j in range(last):
                x_copy(m, l, j).wait_send()
            x_own(m, l).wait_send()

        @pl.when(outer != tp)
        def _():
            o_gather(l).wait_send()

        for j in range(n_tp):
            @pl.when(goes_up)
            def _():
                o_hop(l, j, 0, sp + PAIR).wait_send()

            @pl.when(goes_down)
            def _():
                o_hop(l, j, 1, sp - PAIR).wait_send()

            o_hop(l, j, 2, x_peer).wait_send()

        return carry

    lax.fori_loop(0, layers, drain, 0)

    @pl.when(sp < n_sp - 1)
    def _():
        before_copy().wait_send()

    for c in range(n_chunks):
        store_rows(c).wait()


def fused_shards(n_sp, n_tp, inputs, norm_gain, w_value, w_gate, conv_taps, ln_gain, ln_bias, w_out):
    layers, depth, chan = w_value.shape
    rows, dblk = inputs.shape
    width = w_out.shape[2]
    n_chunks = rows // CHUNK
    features = dblk * n_tp
    ext = HALO * layers
    bf16, f32 = jnp.bfloat16, jnp.float32
    dma = pltpu.SemaphoreType.DMA
    place = pl.BlockSpec(memory_space=pl.ANY)
    return pl.pallas_call(
        functools.partial(fused_kernel, n_sp, n_tp, 1e-06),
        out_shape=jax.ShapeDtypeStruct((rows, dblk), bf16),
        in_specs=[place] * 8,
        out_specs=place,
        scratch_shapes=[
            pltpu.VMEM(norm_gain.shape, f32),
            pltpu.VMEM(conv_taps.shape, f32),
            pltpu.VMEM(ln_gain.shape, f32),
            pltpu.VMEM(ln_bias.shape, f32),
            pltpu.VMEM((rows, dblk), bf16),
            pltpu.VMEM((layers, n_sp * depth, chan), bf16),
            pltpu.VMEM((layers, n_sp * depth, chan), bf16),
            pltpu.VMEM((layers, PAIR, n_tp * chan, width), bf16),
            pltpu.VMEM((n_tp, ext + rows, dblk), bf16),
            pltpu.VMEM((CHUNK, features), bf16),
            pltpu.VMEM((chan // LANES, HALO + ext + rows, LANES), f32),
            pltpu.VMEM((ext + rows, chan), f32),
            pltpu.VMEM((layers, n_chunks, n_tp, 16, CHUNK), f32),
            pltpu.VMEM((n_tp, ext + rows, chan), bf16),
            dma((layers, PAIR, n_sp)),
            dma((layers, PAIR, n_sp // PAIR + 1)),
            dma((layers, PAIR, n_sp // PAIR)),
            dma((layers, n_tp, PAIR)),
            dma((layers, n_tp, 3)),
            dma((layers,)),
            dma((3, n_chunks)),
            dma((3, n_chunks)),
            dma((1,)),
            dma((1,)),
            dma((n_chunks, n_tp)),
            dma((n_chunks, n_tp)),
            dma((3, n_chunks)),
            dma((3, n_chunks)),
            dma((3, layers)),
            dma((5,)),
            dma((n_chunks,)),
        ],
        compiler_params=pltpu.CompilerParams(collective_id=0, has_side_effects=True),
    )(
        inputs,
        norm_gain,
        w_value,
        w_gate,
        conv_taps,
        ln_gain,
        ln_bias,
        w_out,
    )


def fits_kernel(n_sp, n_tp, inputs, w_value, conv_taps, w_out):
    rows, dblk = inputs.shape
    width = w_out.shape[2]
    return (
        n_sp == 4 * PAIR
        and n_tp == PAIR * PAIR
        and rows % CHUNK == 0
        and rows // CHUNK >= 4
        and w_value.shape[0] >= 2
        and w_value.shape[1] % LANES == 0
        and w_value.shape[2] % LANES == 0
        and width % LANES == 0
        and dblk == PAIR * width
        and conv_taps.shape[1] - 1 <= HALO
        and HALO * w_value.shape[0] <= CHUNK
        and rows // CHUNK == 4
    )


def shards(inputs, norm_gain, w_value, w_gate, conv_taps, ln_gain, ln_bias, w_out):
    n_sp, n_tp = lax.axis_size("sp"), lax.axis_size("tp")
    args = (inputs, norm_gain, w_value, w_gate, conv_taps, ln_gain, ln_bias, w_out)
    if fits_kernel(n_sp, n_tp, inputs, w_value, conv_taps, w_out):
        return fused_shards(n_sp, n_tp, *args)
    return plain_shards(*args)


def from_behind(block, axis, distance):
    devices = range(lax.axis_size(axis))
    route = [(i - distance, i) for i in devices if i - distance in devices]
    return lax.ppermute(block, axis, route)


def plain_shards(inputs, norm_gain, w_value, w_gate, conv_taps, ln_gain, ln_bias, w_out):
    rows = inputs.shape[0]
    reach = conv_taps.shape[1] - 1
    layers = conv_taps.shape[0]
    channels = conv_taps.shape[2] * lax.axis_size("tp")
    whole_value, whole_gate, whole_out = (
        lax.all_gather(w_value, "sp", axis=1, tiled=True),
        lax.all_gather(w_gate, "sp", axis=1, tiled=True),
        lax.all_gather(w_out, "sp", axis=2, tiled=True),
    )
    stream = inputs
    for layer in range(layers):
        full_rows = lax.all_gather(stream, "tp", axis=1, tiled=True)
        xf = full_rows.astype(jnp.float32)
        meansq = jnp.mean(xf * xf, axis=1, keepdims=True)
        hidden = (xf * lax.rsqrt(meansq + 1e-06) * norm_gain[layer][None, :]).astype(jnp.bfloat16)
        value = jnp.dot(hidden, whole_value[layer], preferred_element_type=jnp.float32)
        gate = jnp.dot(hidden, whole_gate[layer], preferred_element_type=jnp.float32)
        glu = (value * jax.nn.sigmoid(gate)).astype(jnp.bfloat16)
        rim = from_behind(glu[rows - reach :], "sp", 1)
        padded = jnp.concatenate([rim, glu], axis=0)
        count = padded.shape[0] - reach
        filtered = jnp.zeros((count, glu.shape[1]), jnp.float32)
        for tap in range(reach + 1):
            filtered = filtered + conv_taps[layer, tap][None, :] * padded[tap : tap + count].astype(
                jnp.float32
            )
        total_sum, total_sq = lax.psum(
            (jnp.sum(filtered, axis=1), jnp.sum(filtered * filtered, axis=1)), "tp"
        )
        mean_val = (total_sum / channels)[:, None]
        var_val = (total_sq / channels)[:, None] - mean_val * mean_val
        normed = jax.nn.silu(
            (filtered - mean_val) * lax.rsqrt(var_val + 1e-06) * ln_gain[layer][None, :]
            + ln_bias[layer][None, :]
        ).astype(jnp.bfloat16)
        partial_out = jnp.dot(normed, whole_out[layer], preferred_element_type=jnp.float32)
        summed = lax.psum_scatter(
            partial_out.astype(jnp.bfloat16), "tp", scatter_dimension=1, tiled=True
        ).astype(jnp.float32)
        kept = stream.astype(jnp.float32)
        stream = (kept + summed).astype(jnp.bfloat16)
    return stream


def solution(mesh):
    in_specs = (
        P("sp", "tp"),
        P(),
        P(None, "sp", "tp"),
        P(None, "sp", "tp"),
        P(None, None, "tp"),
        P(None, "tp"),
        P(None, "tp"),
        P(None, "tp", "sp"),
    )
    out_specs = P("sp", "tp")
    return jax.shard_map(shards, mesh=mesh, in_specs=in_specs, out_specs=out_specs, check_vma=False)
```

time: 127 us -> 114 us (0.90)
  the two profiles are of different devices: /device:TPU:3 before, /device:TPU:25 now
where the time goes in v2:
time: 114 us
  Pallas kernels  112 us (98%)
  local copies, waits for them, and re-layouts  1.87 us (2%)
    pallas_call x1, Pallas kernels, fused_shards(): pl.pallas_call(functools.partial(fused_kernel, n_sp, n_tp, 1e-06), out_sh...  112 us

profile of v2, /device:TPU:25, one launch (start us, length us, event | category | flops | bytes accessed | tf_op | source)
XLA Modules:
  0.0 113.5 jit_solution(10094389344896227053)
XLA Ops:
  0.0 111.7 %shard_map.82 = bf16[512,512]{1,0:T(8,128)(2,1)} custom-call(bf16[512,512]{1,0:T(8,128)(2,1)} %x_ref.1, f32[3,2048]{1,0:T(4,128)} %gain_hbm.1, bf16[3,256,256]{2,1,0:T(8,128)(2,1)} %wv_ref.1, bf16[3,256,256]{2,1,0:T(8,128)(2,1)} %wg_ref.1, f32[3,31,256]{2,1,0:T(8,128)} %taps_hbm.1, f32[3,256]{1,0:T(4,128)} %lng_hbm.1, f32[3,256]{1,0:T(4,128)} %lnb_hbm.1, ...), custom_call_target="tpu_custom_call" | custom-call | tf_op jit(solution)/shard_map/pallas_call | solution.py:678
  111.7 1.9 %copy.10 = bf16[512,512]{1,0:T(8,128)(2,1)} copy(bf16[512,512]{1,0:T(8,128)(2,1)} %shard_map.82) | data formatting | bytes 1048576

commit v3 on v2

--- a/solution.py
+++ b/solution.py
@@ -15,7 +15,7 @@
 V, G, O, UP, OVER, ZOWN, XOWN, BEFORE, SIDE = 0, 1, 2, 3, 4, 5, 6, 7, 8
 OWN_X = ((XOWN, V, 1), (XOWN, G, 1))
 OWN_Z = ((ZOWN, V, 1), (ZOWN, G, 1))
-RISEN, FIRST = -1, -2
+FIRST, MIDDLE, RISEN, CLOSING = 0, 1, 2, 3
 LAST_X = ((XOWN, V, 2), (XOWN, G, 2))
 LAST_Z = ((ZOWN, V, 2), (ZOWN, G, 2))
 
@@ -41,26 +41,27 @@
     *every(O, 0), *OWN_Z, *OWN_X,
 )
 END_PLAN = {
-    1: ((O, 0, RISEN), (O, 1, 0)), 2: ((O, 2, 0), (XOWN, G, 1)), 3: ((O, 3, 0),), 5: ((V, 0, 1), *LAST_Z),
-    6: ((V, 1, 1),), 7: ((V, 2, 1),), 8: ((G, 0, 1), (SIDE, 0, 1)), 9: ((G, 1, 1),), 10: ((G, 2, 1),),
-    12: ((XOWN, V, 2),),
+    1: ((O, 0, 0, RISEN), (O, 1, 0)), 2: ((O, 2, 0),), 3: ((O, 3, 0), (XOWN, G, 1)), 4: ((V, 0, 1), *LAST_Z),
+    13: ((G, 0, 1, FIRST), (V, 1, 1, FIRST), (V, 2, 1, FIRST)),
+    6: ((V, 1, 1, RISEN),), 7: ((V, 2, 1, RISEN), (SIDE, V, 1)), 8: ((G, 0, 1, RISEN), (SIDE, G, 1)),
+    9: ((G, 1, 1),), 10: ((G, 2, 1),), 12: ((XOWN, V, 2),),
 }
 HEAD_PLAN = {
-    3: every(UP, 1), 5: ((V, 0, 1), *LAST_Z), 6: ((V, 1, 1),), 7: ((V, 2, 1),),
-    8: ((G, 0, 1), (SIDE, 0, 1)), 9: ((G, 1, 1),), 10: ((G, 2, 1), *every(OVER, 1), *LAST_X),
+    3: every(UP, 1), 5: ((V, 0, 1), *LAST_Z), 6: ((V, 1, 1),), 7: ((V, 2, 1), (SIDE, V, 1)),
+    8: ((G, 0, 1), (SIDE, G, 1)), 9: ((G, 1, 1),), 10: ((G, 2, 1), *every(OVER, 1), *LAST_X),
 }
 MID_PLAN = {
-    1: ((O, 3, FIRST), (ZOWN, G, 1), *OWN_X), 3: ((V, 0, 1),), 4: ((V, 1, 1), (V, 2, 1)),
-    5: ((G, 0, 1),), 6: ((G, 1, 1),), 7: ((G, 2, 1), (SIDE, 0, 1)),
+    1: ((O, 3, 0, FIRST), (ZOWN, G, 1), *OWN_X), 2: ((V, 0, 1), (V, 1, 1)), 3: ((V, 2, 1),), 4: ((G, 0, 1), (SIDE, V, 1)),
+    5: ((G, 1, 1),), 6: ((G, 2, 1),), 7: ((SIDE, G, 1),),
     9: ((O, 0, 1),), 10: ((O, 1, 1),), 11: ((O, 2, 1),), 12: ((O, 3, 1), (ZOWN, V, 2)),
 }
 ROOT_PLAN = {
-    1: ((V, 0, 1),), 2: ((V, 1, 1),), 3: ((V, 2, 1),), 4: ((G, 0, 1),), 5: ((G, 1, 1),),
-    6: ((G, 2, 1),), 7: ((SIDE, 0, 1), (O, 0, 1), (O, 1, 1)), 8: ((O, 2, 1), (O, 3, 1), *LAST_Z, *LAST_X),
+    1: ((V, 0, 1),), 2: ((V, 1, 1),), 3: ((V, 2, 1),), 4: ((G, 0, 1),), 5: ((G, 1, 1), (SIDE, V, 1)),
+    6: ((G, 2, 1),), 7: ((SIDE, G, 1), (O, 0, 1), (O, 1, 1)), 8: ((O, 2, 1), (O, 3, 1), *LAST_Z, *LAST_X),
 }
 NEXT_PLAN = {
-    1: ((V, 0, 1),), 2: ((V, 1, 1),), 3: ((V, 2, 1),), 4: ((G, 0, 1), (UP, 0, 1)), 5: ((G, 1, 1), (UP, 1, 1)),
-    6: ((G, 2, 1), (UP, 2, 1)), 7: ((SIDE, 0, 1), (UP, 3, 1)),
+    1: ((V, 0, 1),), 2: ((V, 1, 1),), 3: ((V, 2, 1),), 4: ((G, 0, 1), (UP, 0, 1)), 5: ((G, 1, 1), (UP, 1, 1), (SIDE, V, 1)),
+    6: ((G, 2, 1), (UP, 2, 1)), 7: ((SIDE, G, 1), (UP, 3, 1)),
     8: (*every(OVER, 1), *LAST_Z, *LAST_X),
 }
 
@@ -70,7 +71,7 @@
     x_ref, gain_hbm, wv_ref, wg_ref, taps_hbm, lng_hbm, lnb_hbm, wo_ref,
     out_ref,
     gain_ref, taps_ref, lng_ref, lnb_ref, out_all, wv_all, wg_all, wo_all, xf, hid, glu, filt, stat, nrm,
-    w_recv, w_zsend, w_xsend, o_recv, o_send, og_send,
+    w_recv, w_xrecv, w_zsend, w_xsend, o_recv, o_xrecv, o_send, og_send,
     ag_recv, ag_send, before_s, before_r, st_recv, st_send, nr_recv, nr_send,
     in_sem, small_sem, out_sem,
 ):
@@ -197,35 +198,38 @@
 
     def z_copy(m, l, j):
         to = line(j) * PAIR + inner
-        return remote(w_slot(m, l, sp), w_slot(m, l, sp), w_zsend.at[l, m, j], w_recv.at[l, m, sp], to, tp)
+        return remote(w_slot(m, l, sp), w_slot(m, l, sp), w_zsend.at[m], w_recv.at[l, m, outer], to, tp)
 
     def z_arrival(m, l, j):
         s = line(j) * PAIR + inner
-        return remote(w_slot(m, l, s), w_slot(m, l, s), w_zsend.at[l, m, j], w_recv.at[l, m, s], s, tp)
+        return remote(w_slot(m, l, s), w_slot(m, l, s), w_zsend.at[m], w_recv.at[l, m, line(j)], s, tp)
 
     def z_forward(m, l, j):
         s = line(j) * PAIR + inner
         to = line(1 if j == 0 else 0) * PAIR + inner
         slot = w_slot(m, l, s)
-        return remote(slot, slot, w_zsend.at[l, m, PAIR + j], w_recv.at[l, m, s], to, tp)
+        return remote(slot, slot, w_zsend.at[m], w_recv.at[l, m, line(j)], to, tp)
 
     def x_own(m, l):
-        return remote(w_slot(m, l, sp), w_slot(m, l, sp), w_xsend.at[l, m, last], w_recv.at[l, m, sp], x_peer, tp)
+        return remote(w_slot(m, l, sp), w_slot(m, l, sp), w_xsend.at[m], w_xrecv.at[l, m, 0], x_peer, tp)
 
     def x_copy(m, l, j):
         s = line(j) * PAIR + inner
         slot = w_slot(m, l, s)
-        return remote(slot, slot, w_xsend.at[l, m, j], w_recv.at[l, m, s], x_peer, tp)
-
-    def x_arrival(m, l, z):
-        s = z * PAIR + (PAIR - 1 - inner)
-        slot = w_slot(m, l, s)
-        return remote(slot, slot, w_xsend.at[l, m, last], w_recv.at[l, m, s], x_peer, tp)
+        return remote(slot, slot, w_xsend.at[m], w_xrecv.at[l, m, 1], x_peer, tp)
+
+    def x_arrival(m, l):
+        slot = w_slot(m, l, x_peer)
+        return remote(slot, slot, w_xsend.at[m], w_xrecv.at[l, m, 0], x_peer, tp)
+
+    def x_arrivals(m, l):
+        block = (wv_all, wg_all)[m].at[l, pl.ds(0, last * depth), :]
+        return remote(block, block, w_xsend.at[m], w_xrecv.at[l, m, 1], x_peer, tp)
 
     def side_copy(m, l):
         to = line(0) * PAIR + inner
         slot = w_slot(m, l, x_peer)
-        return remote(slot, slot, w_xsend.at[l, m, 0], w_recv.at[l, m, x_peer], to, tp)
+        return remote(slot, slot, w_xsend.at[m], w_xrecv.at[l, m, 1], to, tp)
 
     def z_own(m, l):
         z_copy(m, l, 0).start()
@@ -243,32 +247,38 @@
 
         if j or not side:
             x_copy(m, l, j).start()
+        elif m == V:
+            @pl.when(jnp.logical_not(by_side(m, l)))
+            def _():
+                x_copy(m, l, j).start()
+
+    def by_side(m, l):
+        return l > 0 if m == G else (l > 0) & ((l < layers - 1) | (upper == far_half))
 
     def relay_side(m, l):
-        x_arrival(m, l, outer).wait_recv()
-        side_copy(m, l).start()
+        @pl.when(by_side(m, l))
+        def _():
+            x_arrival(m, l).wait_recv()
+            side_copy(m, l).start()
 
     def w_ready(m, l):
-        if m == 1:
-            @pl.when(l == 0)
-            def _():
-                x_arrival(m, l, outer).wait_recv()
-        else:
-            x_arrival(m, l, outer).wait_recv()
-        for j in range(last):
-            x_arrival(m, l, line(j)).wait_recv()
+        @pl.when(jnp.logical_not(by_side(m, l)))
+        def _():
+            x_arrival(m, l).wait_recv()
+
+        x_arrivals(m, l).wait_recv()
 
     def o_gather(l):
-        return remote(wo_ref.at[l], o_slot(l, inner, tp), og_send.at[l], o_recv.at[l, tp, inner], sp, outer)
+        return remote(wo_ref.at[l], o_slot(l, inner, tp), og_send.at[0], o_recv.at[l, tp], sp, outer)
 
     def o_hop(l, j, way, to):
         b = lax.rem(tp + j, n_tp)
         slot = o_slot(l, inner, b)
-        return remote(slot, slot, o_send.at[l, j, way], o_recv.at[l, b, inner], to, tp)
-
-    def o_arrival(l, b, x):
-        slot = o_slot(l, x, b)
-        return remote(slot, slot, o_send.at[l, 0, 0], o_recv.at[l, b, x], x_peer, tp)
+        return remote(slot, slot, o_send.at[way], o_xrecv.at[l] if way == 2 else o_recv.at[l, b], to, tp)
+
+    def o_arrival(l, b):
+        slot = o_slot(l, inner, b)
+        return remote(slot, slot, o_send.at[0], o_recv.at[l, b], x_peer, tp)
 
     goes_up = (outer >= tp) & (outer < last)
     goes_down = (outer <= tp) & (outer > 0)
@@ -282,9 +292,9 @@
         if j == 0:
             @pl.when(outer != tp)
             def _():
-                o_arrival(l, tp, inner).wait_recv()
+                o_arrival(l, tp).wait_recv()
         else:
-            o_arrival(l, lax.rem(tp + j, n_tp), inner).wait_recv()
+            o_arrival(l, lax.rem(tp + j, n_tp)).wait_recv()
 
     def o_along(l, j):
         @pl.when(goes_up)
@@ -303,40 +313,40 @@
             o_hop(l, j, 2, x_peer).start()
 
     def o_ready(l):
-        for j in range(n_tp):
-            o_arrival(l, lax.rem(tp + j, n_tp), PAIR - 1 - inner).wait_recv()
+        block = wo_all.at[l, 0]
+        remote(block, block, o_send.at[2], o_xrecv.at[l], x_peer, tp).wait_recv()
 
     def ag_far(c, l):
         r = chunk_rows(c, l)
-        return remote(xf.at[tp, r, :], xf.at[tp, r, :], ag_send.at[0, c], ag_recv.at[0, c], sp, far)
+        return remote(xf.at[tp, r, :], xf.at[tp, r, :], ag_send.at[c], ag_recv.at[0, c], sp, far)
 
     def ag_partner(c, l):
         r = chunk_rows(c, l)
-        return remote(xf.at[tp, r, :], xf.at[tp, r, :], ag_send.at[1, c], ag_recv.at[1, c], sp, partner)
+        return remote(xf.at[tp, r, :], xf.at[tp, r, :], ag_send.at[c], ag_recv.at[1, c], sp, partner)
 
     def ag_forward(c, l):
         r = chunk_rows(c, l)
-        return remote(xf.at[far, r, :], xf.at[far, r, :], ag_send.at[2, c], ag_recv.at[2, c], sp, partner)
+        return remote(xf.at[far, r, :], xf.at[far, r, :], ag_send.at[c], ag_recv.at[1, c], sp, partner)
 
     def nr_far(c, l):
         r = chunk_rows(c, l + 1)
-        return remote(nrm.at[tp, r, :], nrm.at[tp, r, :], nr_send.at[0, c], nr_recv.at[0, c], sp, far)
+        return remote(nrm.at[tp, r, :], nrm.at[tp, r, :], nr_send.at[c], nr_recv.at[0, c], sp, far)
 
     def nr_partner(c, l):
         r = chunk_rows(c, l + 1)
-        return remote(nrm.at[tp, r, :], nrm.at[tp, r, :], nr_send.at[1, c], nr_recv.at[1, c], sp, partner)
+        return remote(nrm.at[tp, r, :], nrm.at[tp, r, :], nr_send.at[c], nr_recv.at[1, c], sp, partner)
 
     def nr_forward(c, l):
         r = chunk_rows(c, l + 1)
-        return remote(nrm.at[far, r, :], nrm.at[far, r, :], nr_send.at[2, c], nr_recv.at[2, c], sp, partner)
+        return remote(nrm.at[far, r, :], nrm.at[far, r, :], nr_send.at[c], nr_recv.at[1, c], sp, partner)
 
     def stat_copy(l, c, step):
         to = lax.rem(tp + step, n_tp)
-        return remote(stat.at[l, c, tp, stat_rows(c), :], stat.at[l, c, tp, stat_rows(c), :], st_send.at[c, step], st_recv.at[c, tp], sp, to)
-
-    def stat_arrival(l, c, step):
-        src = lax.rem(tp + step, n_tp)
-        return remote(stat.at[l, c, src, stat_rows(c), :], stat.at[l, c, src, stat_rows(c), :], st_send.at[c, step], st_recv.at[c, src], sp, src)
+        return remote(stat.at[l, c, tp, stat_rows(c), :], stat.at[l, c, tp, stat_rows(c), :], st_send.at[c], st_recv.at[c], sp, to)
+
+    def stats(l, c):
+        block = stat.at[l, c, pl.ds(0, n_tp - 1), stat_rows(c), :]
+        return remote(block, block, st_send.at[c], st_recv.at[c], sp, far)
 
     def before_copy():
         to = lax.rem(sp + 1, n_sp)
@@ -358,16 +368,15 @@
 
     def ag_sent(l, c):
         def go(k):
-            ag_far(c, k).wait_send()
-            ag_partner(c, k).wait_send()
-            ag_forward(c, k).wait_send()
+            block = xf.at[pl.ds(0, 3), chunk_rows(c, k), :]
+            remote(block, block, ag_send.at[c], ag_recv.at[1, c], sp, far).wait_send()
 
         by_layer(c, l, go)
 
     def ag_wait(l, c):
         def go(k):
-            ag_partner(c, k).wait_recv()
-            ag_forward(c, k).wait_recv()
+            block = xf.at[pl.ds(0, PAIR), chunk_rows(c, k), :]
+            remote(block, block, ag_send.at[c], ag_recv.at[1, c], sp, partner).wait_recv()
 
         by_layer(c, l, go)
 
@@ -380,22 +389,23 @@
 
     def nr_sent(l, c):
         def go(k):
-            nr_far(c, k).wait_send()
-            nr_partner(c, k).wait_send()
-            nr_forward(c, k).wait_send()
+            block = nrm.at[pl.ds(0, 3), chunk_rows(c, k + 1), :]
+            remote(block, block, nr_send.at[c], nr_recv.at[1, c], sp, far).wait_send()
 
         by_layer(c, l, go)
 
     def nr_wait(l, c):
         def go(k):
-            nr_partner(c, k).wait_recv()
-            nr_forward(c, k).wait_recv()
+            block = nrm.at[pl.ds(0, PAIR), chunk_rows(c, k + 1), :]
+            remote(block, block, nr_send.at[c], nr_recv.at[1, c], sp, partner).wait_recv()
 
         by_layer(c, l, go)
 
-    def do_glu(l, c):
-        ag_wait(l, c)
-        for start, size in parts(c):
+    def do_glu(l, cs):
+        for c in cs:
+            ag_wait(l, c)
+
+        def glu_part(start, size):
             r = slice(start, start + size)
             blocks = [xf[b, r, :].astype(jnp.float32) for b in range(n_tp)]
             total = sum(jnp.sum(b * b, axis=1, keepdims=True) for b in blocks)
@@ -409,12 +419,20 @@
             gate = jnp.dot(h, wg_all[l], preferred_element_type=jnp.float32)
             g = (value * jax.nn.sigmoid(gate)).astype(jnp.bfloat16).astype(jnp.float32)
             if start < ext:
-                g = jnp.where(sp > 0, g, 0.0)
+                row = lax.broadcasted_iota(jnp.int32, g.shape, 0)
+                g = jnp.where((row >= ext - start) | (sp > 0), g, 0.0)
             for k in range(halves):
                 glu[k, HALO + start:HALO + start + size, :] = g[:, k * LANES:(k + 1) * LANES]
 
+        start, size = ext + cs[0] * CHUNK, len(cs) * CHUNK
+        if cs[0]:
+            glu_part(start, size)
+        else:
+            pl.when(l < layers - 1)(functools.partial(glu_part, 0, start + size))
+            pl.when(l == layers - 1)(functools.partial(glu_part, ext - HALO, HALO + size))
+
     def do_conv(l, c):
-        for i, (start, size) in enumerate(parts(c)):
+        def conv_part(i, start, size):
             sums = jnp.zeros((size, 1), jnp.float32)
             squares = jnp.zeros((size, 1), jnp.float32)
             for k in range(halves):
@@ -430,12 +448,18 @@
             if size < CHUNK:
                 both = jnp.concatenate([both, jnp.zeros((CHUNK - size, LANES), jnp.float32)], axis=0)
             stat[l, c, tp, 8 * i:8 * i + 8, :] = jnp.transpose(both)[0:8, :]
+
+        for i, (start, size) in enumerate(parts(c)):
+            if start < ext:
+                pl.when(l < layers - 1)(functools.partial(conv_part, i, start, size))
+            else:
+                conv_part(i, start, size)
         for step in range(1, n_tp):
             stat_copy(l, c, step).start()
 
     def do_norm(l, c):
-        for step in range(1, n_tp):
-            stat_arrival(l, c, step).wait_recv()
+        stats(l, c).wait_recv()
+
         def norm_part(i, start, size):
             r = slice(start, start + size)
             tot = stat[l, c, 0, 8 * i:8 * i + 8, :]
@@ -450,8 +474,7 @@
         for i, (start, size) in enumerate(parts(c)):
             pl.when((start >= ext) | (l < layers - 1))(functools.partial(norm_part, i, start, size))
         ag_sent(l, c)
-        for step in range(1, n_tp):
-            stat_copy(l, c, step).wait_send()
+        stats(l, c).wait_send()
         nr_start(l, c)
 
     def do_hand(l, c):
@@ -465,30 +488,30 @@
         r = pl.ds(c * CHUNK, CHUNK)
         return pltpu.make_async_copy(out_all.at[r, :], out_ref.at[r, :], out_sem.at[c])
 
-    def do_out(l, c):
+    def do_half(l, c, q, final):
+        for start, size in parts(c):
+            if final and start < ext:
+                continue
+            r = slice(start, start + size)
+            cols = pl.ds(pl.multiple_of(q * width, width), width)
+            full = jnp.concatenate([nrm[b, r, :] for b in range(n_tp)], axis=1)
+            branch = jnp.dot(full, wo_all[l, q], preferred_element_type=jnp.float32)
+            new = (xf[tp, r, cols].astype(jnp.float32) + branch).astype(jnp.bfloat16)
+            if final:
+                out_all[start - ext:start - ext + size, cols] = new
+            else:
+                xf[tp, r, cols] = new
+
+    def do_near(l, c, final):
         nr_wait(l, c)
-        def out_part(start, size):
-            r = slice(start, start + size)
-            full = jnp.concatenate([nrm[b, r, :] for b in range(n_tp)], axis=1)
-            for q in range(PAIR):
-                cols = slice(q * width, (q + 1) * width)
-                branch = jnp.dot(full, wo_all[l, q], preferred_element_type=jnp.float32)
-                new = (xf[tp, r, cols].astype(jnp.float32) + branch).astype(jnp.bfloat16)
-                xf[tp, r, cols] = new
-                if start >= ext:
-                    out_all[start - ext:start - ext + size, cols] = new
-
-        for start, size in parts(c):
-            pl.when((start >= ext) | (l < layers - 1))(functools.partial(out_part, start, size))
-
-        @pl.when(l < layers - 1)
-        def _():
+        do_half(l, c, inner, final)
+
+    def do_rest(l, c, final):
+        do_half(l, c, PAIR - 1 - inner, final)
+        if final:
+            store_rows(c).start()
+        else:
             ag_start(l + 1, c)
-
-        @pl.when(l == layers - 1)
-        def _():
-            store_rows(c).start()
-
         nr_sent(l, c)
 
     by_head = near_end * (outer - tp) * (outer - tp) * (1 - (far_half - core) * (far_half - core)) == 1
@@ -510,7 +533,7 @@
 
             ag_start(0, 0)
         elif kind == SIDE:
-            relay_side(G, l)
+            relay_side(j, l)
         elif kind == ZOWN:
             z_own(j, l)
         elif kind == XOWN:
@@ -518,7 +541,7 @@
         elif kind >= O:
             relay_o(l, j, kind)
         else:
-            relay_piece(kind, l, j, side and kind == G)
+            relay_piece(kind, l, j, side)
 
     for m in (V, G):
         z_own(m, 0)
@@ -542,6 +565,7 @@
 
     for small in smalls:
         small.wait()
+    send_o(1)
     for role, order, _ in roles:
         @pl.when(role)
         def _():
@@ -561,50 +585,70 @@
 
         def slot(n):
             for role, _, plan in roles:
-                for kind, j, later in plan.get(n, ()):
-                    if later == RISEN:
-                        when = role & (l > 0)
-                    elif later == FIRST:
-                        when = role & (l == 0)
-                    else:
-                        when = (role & (l + later < layers)) if later else role
+                for kind, j, later, *turn in plan.get(n, ()):
+                    when = (role & (l + later < layers)) if later else role
+                    for t in turn:
+                        when = when & (l == 0, (l > 0) & (l < layers - 1), l > 0, l == layers - 2)[t]
 
                     @pl.when(when)
                     def _():
-                        act(kind, j, l + max(later, 0), True)
+                        act(kind, j, l + later, True)
 
         def pass_next(c):
             ahead(lambda: do_pass(l + 1, c))
 
-        do_glu(l, 0)
+        do_glu(l, (0, 1))
         do_conv(l, 0)
-        ahead(lambda: send_o(l + 1))
         slot(1)
-        do_glu(l, 1)
         do_conv(l, 1)
-        do_glu(l, 2)
+        do_glu(l, (2, 3))
         do_conv(l, 2)
         slot(2)
         do_norm(l, 0)
-        do_glu(l, 3)
         do_conv(l, 3)
         do_norm(l, 1)
         slot(3)
         do_norm(l, 2)
         do_norm(l, 3)
         slot(4)
-        do_hand(l, 0)
-        slot(5)
-        do_hand(l, 1)
-        o_ready(l)
-        do_out(l, 0)
-        do_hand(l, 2)
-        do_out(l, 1)
-        slot(6)
-        do_hand(l, 3)
-        do_out(l, 2)
-        slot(7)
-        do_out(l, 3)
+        @pl.when(more)
+        def _():
+            do_hand(l, 0)
+            slot(5)
+            do_hand(l, 1)
+            slot(13)
+            o_ready(l)
+            do_near(l, 0, False)
+            do_rest(l, 0, False)
+            do_hand(l, 2)
+            do_near(l, 1, False)
+            do_rest(l, 1, False)
+            slot(6)
+            do_hand(l, 3)
+            do_near(l, 2, False)
+            do_rest(l, 2, False)
+            slot(7)
+            do_near(l, 3, False)
+            do_rest(l, 3, False)
+
+        @pl.when(l == layers - 1)
+        def _():
+            do_hand(l, 0)
+            do_hand(l, 1)
+            do_near(l, 0, True)
+            do_hand(l, 2)
+            do_near(l, 1, True)
+            do_hand(l, 3)
+            do_near(l, 2, True)
+            do_near(l, 3, True)
+            o_ready(l)
+            for c in range(n_chunks):
+                do_rest(l, c, True)
+
+        @pl.when(l < layers - 2)
+        def _():
+            send_o(l + 2)
+
         slot(8)
         pass_next(0)
         slot(9)
@@ -624,38 +668,34 @@
 
     lax.fori_loop(0, layers, layer_body, 0)
 
-    def drain(l, carry):
-        for m in range(PAIR):
-            z_copy(m, l, 0).wait_send()
-
-            @pl.when(near_end == 1)
-            def _():
-                z_copy(m, l, 1).wait_send()
-                for j in range(last):
-                    z_forward(m, l, j).wait_send()
-
-            for j in range(last):
-                x_copy(m, l, j).wait_send()
-            x_own(m, l).wait_send()
-
-        @pl.when(outer != tp)
-        def _():
-            o_gather(l).wait_send()
-
-        for j in range(n_tp):
-            @pl.when(goes_up)
-            def _():
-                o_hop(l, j, 0, sp + PAIR).wait_send()
-
-            @pl.when(goes_down)
-            def _():
-                o_hop(l, j, 1, sp - PAIR).wait_send()
-
-            o_hop(l, j, 2, x_peer).wait_send()
-
-        return carry
-
-    lax.fori_loop(0, layers, drain, 0)
+    def sent(block, sem):
+        remote(block, block, sem, before_r.at[0], x_peer, tp).wait_send()
+
+    for m in range(PAIR):
+        whole = (wv_all, wg_all)[m]
+        sent(whole.at[:, pl.ds(0, n_out * depth), :], w_xsend.at[m])
+
+        @pl.when(near_end == 0)
+        def _():
+            sent(whole.at[:, pl.ds(0, depth), :], w_zsend.at[m])
+
+        @pl.when(near_end == 1)
+        def _():
+            sent(whole.at[:, pl.ds(0, (PAIR + last) * depth), :], w_zsend.at[m])
+
+    @pl.when(outer != tp)
+    def _():
+        sent(wo_all.at[:, 0, pl.ds(0, chan), :], og_send.at[0])
+
+    @pl.when(goes_up)
+    def _():
+        sent(wo_all.at[:, 0], o_send.at[0])
+
+    @pl.when(goes_down)
+    def _():
+        sent(wo_all.at[:, 0], o_send.at[1])
+
+    sent(wo_all.at[:, 0], o_send.at[2])
 
     @pl.when(sp < n_sp - 1)
     def _():
@@ -690,25 +730,27 @@
             pltpu.VMEM((layers, n_sp * depth, chan), bf16),
             pltpu.VMEM((layers, PAIR, n_tp * chan, width), bf16),
             pltpu.VMEM((n_tp, ext + rows, dblk), bf16),
-            pltpu.VMEM((CHUNK, features), bf16),
+            pltpu.VMEM((ext + PAIR * CHUNK, features), bf16),
             pltpu.VMEM((chan // LANES, HALO + ext + rows, LANES), f32),
             pltpu.VMEM((ext + rows, chan), f32),
             pltpu.VMEM((layers, n_chunks, n_tp, 16, CHUNK), f32),
             pltpu.VMEM((n_tp, ext + rows, chan), bf16),
-            dma((layers, PAIR, n_sp)),
-            dma((layers, PAIR, n_sp // PAIR + 1)),
             dma((layers, PAIR, n_sp // PAIR)),
-            dma((layers, n_tp, PAIR)),
-            dma((layers, n_tp, 3)),
+            dma((layers, PAIR, 2)),
+            dma((PAIR,)),
+            dma((PAIR,)),
+            dma((layers, n_tp)),
             dma((layers,)),
-            dma((3, n_chunks)),
-            dma((3, n_chunks)),
+            dma((3,)),
+            dma((1,)),
+            dma((2, n_chunks)),
+            dma((n_chunks,)),
             dma((1,)),
             dma((1,)),
-            dma((n_chunks, n_tp)),
-            dma((n_chunks, n_tp)),
-            dma((3, n_chunks)),
-            dma((3, n_chunks)),
+            dma((n_chunks,)),
+            dma((n_chunks,)),
+            dma((2, n_chunks)),
+            dma((n_chunks,)),
             dma((3, layers)),
             dma((5,)),
             dma((n_chunks,)),

time: 114 us -> 110 us (0.965)
  the two profiles are of different devices: /device:TPU:25 before, /device:TPU:3 now
where the time goes in v3:
time: 110 us
  Pallas kernels  108 us (98%)
  local copies, waits for them, and re-layouts  1.87 us (2%)
    pallas_call x1, Pallas kernels, fused_shards(): pl.pallas_call(functools.partial(fused_kernel, n_sp, n_tp, 1e-06), out_sh...  108 us

profile of v3, /device:TPU:3, one launch (start us, length us, event | category | flops | bytes accessed | tf_op | source)
XLA Modules:
  0.0 110.0 jit_solution(12375793503258726934)
XLA Ops:
  0.0 108.1 %shard_map.82 = bf16[512,512]{1,0:T(8,128)(2,1)} custom-call(bf16[512,512]{1,0:T(8,128)(2,1)} %x_ref.1, f32[3,2048]{1,0:T(4,128)} %gain_hbm.1, bf16[3,256,256]{2,1,0:T(8,128)(2,1)} %wv_ref.1, bf16[3,256,256]{2,1,0:T(8,128)(2,1)} %wg_ref.1, f32[3,31,256]{2,1,0:T(8,128)} %taps_hbm.1, f32[3,256]{1,0:T(4,128)} %lng_hbm.1, f32[3,256]{1,0:T(4,128)} %lnb_hbm.1, ...), custom_call_target="tpu_custom_call" | custom-call | tf_op jit(solution)/shard_map/pallas_call | solution.py:718
  108.1 1.9 %copy.10 = bf16[512,512]{1,0:T(8,128)(2,1)} copy(bf16[512,512]{1,0:T(8,128)(2,1)} %shard_map.82) | data formatting | bytes 1048576

commit v4 on v3

--- a/solution.py
+++ b/solution.py
@@ -15,7 +15,7 @@
 V, G, O, UP, OVER, ZOWN, XOWN, BEFORE, SIDE = 0, 1, 2, 3, 4, 5, 6, 7, 8
 OWN_X = ((XOWN, V, 1), (XOWN, G, 1))
 OWN_Z = ((ZOWN, V, 1), (ZOWN, G, 1))
-FIRST, MIDDLE, RISEN, CLOSING = 0, 1, 2, 3
+FIRST, EARLY, RISEN, LAST = 0, 1, 2, 3
 LAST_X = ((XOWN, V, 2), (XOWN, G, 2))
 LAST_Z = ((ZOWN, V, 2), (ZOWN, G, 2))
 
@@ -40,8 +40,16 @@
     (V, 0, 0), (V, 1, 0), (G, 0, 0), (G, 1, 0), (V, 2, 0), (BEFORE, 0, 0), (G, 2, 0),
     *every(O, 0), *OWN_Z, *OWN_X,
 )
+SOON_OPEN = (*END_OPEN, (O, 1, 0))
+SOON_PLAN = {
+    1: ((O, 1, 0, RISEN), (O, 2, 0)), 2: ((O, 3, 0),), 3: ((XOWN, V, 1, RISEN), (XOWN, G, 1)), 4: ((V, 0, 1), *LAST_Z),
+    13: ((G, 0, 1, FIRST), (V, 1, 1, FIRST), (V, 2, 1, FIRST)),
+    6: ((V, 1, 1, RISEN),), 7: ((V, 2, 1, RISEN), (SIDE, V, 1)), 8: ((G, 0, 1, RISEN), (SIDE, G, 1)),
+    9: ((G, 1, 1),), 10: ((G, 2, 1),), 12: ((O, 0, 1),),
+}
 END_PLAN = {
-    1: ((O, 0, 0, RISEN), (O, 1, 0)), 2: ((O, 2, 0),), 3: ((O, 3, 0), (XOWN, G, 1)), 4: ((V, 0, 1), *LAST_Z),
+    1: ((O, 0, 0, RISEN), (O, 1, 0, EARLY)), 2: ((O, 2, 0, EARLY), (O, 1, 0, LAST)),
+    3: ((O, 3, 0, EARLY), (XOWN, G, 1), (O, 2, 0, LAST)), 4: ((V, 0, 1), *LAST_Z, (O, 3, 0, LAST)),
     13: ((G, 0, 1, FIRST), (V, 1, 1, FIRST), (V, 2, 1, FIRST)),
     6: ((V, 1, 1, RISEN),), 7: ((V, 2, 1, RISEN), (SIDE, V, 1)), 8: ((G, 0, 1, RISEN), (SIDE, G, 1)),
     9: ((G, 1, 1),), 10: ((G, 2, 1),), 12: ((XOWN, V, 2),),
@@ -506,22 +514,20 @@
         nr_wait(l, c)
         do_half(l, c, inner, final)
 
-    def do_rest(l, c, final):
-        do_half(l, c, PAIR - 1 - inner, final)
-        if final:
-            store_rows(c).start()
-        else:
-            ag_start(l + 1, c)
+    def do_rest(l, c):
+        do_half(l, c, PAIR - 1 - inner, False)
+        ag_start(l + 1, c)
         nr_sent(l, c)
 
     by_head = near_end * (outer - tp) * (outer - tp) * (1 - (far_half - core) * (far_half - core)) == 1
     is_root = (near_end == 1) & (outer == tp)
     is_mid = (near_end == 1) & (outer != tp) & jnp.logical_not(by_head)
     is_head = (near_end == 0) & (outer == tp)
-    is_end = (near_end == 0) & (outer != tp)
+    is_soon = (near_end == 0) & ((outer - tp) * (outer - tp) == 1)
+    is_end = (near_end == 0) & ((outer - tp) * (outer - tp) > 1)
 
     roles = (
-        (is_end, END_OPEN, END_PLAN), (is_head, HEAD_OPEN, HEAD_PLAN),
+        (is_end, END_OPEN, END_PLAN), (is_soon, SOON_OPEN, SOON_PLAN), (is_head, HEAD_OPEN, HEAD_PLAN),
         (is_mid, MID_OPEN, MID_PLAN), (is_root, NEAR_OPEN, ROOT_PLAN), (by_head, NEAR_OPEN, NEXT_PLAN),
     )
 
@@ -588,7 +594,7 @@
                 for kind, j, later, *turn in plan.get(n, ()):
                     when = (role & (l + later < layers)) if later else role
                     for t in turn:
-                        when = when & (l == 0, (l > 0) & (l < layers - 1), l > 0, l == layers - 2)[t]
+                        when = when & (l == 0, l < layers - 1, l > 0, l == layers - 1)[t]
 
                     @pl.when(when)
                     def _():
@@ -597,9 +603,10 @@
         def pass_next(c):
             ahead(lambda: do_pass(l + 1, c))
 
-        do_glu(l, (0, 1))
+        do_glu(l, (0,))
         do_conv(l, 0)
         slot(1)
+        do_glu(l, (1,))
         do_conv(l, 1)
         do_glu(l, (2, 3))
         do_conv(l, 2)
@@ -619,17 +626,17 @@
             slot(13)
             o_ready(l)
             do_near(l, 0, False)
-            do_rest(l, 0, False)
+            do_rest(l, 0)
             do_hand(l, 2)
             do_near(l, 1, False)
-            do_rest(l, 1, False)
+            do_rest(l, 1)
             slot(6)
             do_hand(l, 3)
             do_near(l, 2, False)
-            do_rest(l, 2, False)
+            do_rest(l, 2)
             slot(7)
             do_near(l, 3, False)
-            do_rest(l, 3, False)
+            do_rest(l, 3)
 
         @pl.when(l == layers - 1)
         def _():
@@ -642,8 +649,18 @@
             do_near(l, 2, True)
             do_near(l, 3, True)
             o_ready(l)
+            for c in range(0, n_chunks, PAIR):
+                r = slice(c * CHUNK, (c + PAIR) * CHUNK)
+                q = PAIR - 1 - inner
+                cols = pl.ds(pl.multiple_of(q * width, width), width)
+                x_rows = slice(ext + c * CHUNK, ext + (c + PAIR) * CHUNK)
+                full = jnp.concatenate([nrm[b, x_rows, :] for b in range(n_tp)], axis=1)
+                branch = jnp.dot(full, wo_all[l, q], preferred_element_type=jnp.float32)
+                out_all[r, cols] = (xf[tp, x_rows, cols].astype(jnp.float32) + branch).astype(jnp.bfloat16)
+                for k in range(c, c + PAIR):
+                    store_rows(k).start()
             for c in range(n_chunks):
-                do_rest(l, c, True)
+                nr_sent(l, c)
 
         @pl.when(l < layers - 2)
         def _():

time: 110 us -> 108 us (0.982); the launches traced: 110 us -> 107 us
  Pallas kernels: 108 us -> 105 us
    pallas_call x1, Pallas kernels: 108 us -> 105 us  [fused_shards(): pl.pallas_call(functools.partial(fused_kernel, n_sp, n_tp, 1e-06), out_sh...]
where the time goes in v4:
time: 108 us; the launch traced here: 107 us
  Pallas kernels  105 us (97%)
  local copies, waits for them, and re-layouts  1.87 us (2%)
    pallas_call x1, Pallas kernels, fused_shards(): pl.pallas_call(functools.partial(fused_kernel, n_sp, n_tp, 1e-06), out_sh...  105 us

profile of v4, /device:TPU:3, one launch (start us, length us, event | category | flops | bytes accessed | tf_op | source)
XLA Modules:
  0.0 106.7 jit_solution(10639032603839739367)
XLA Ops:
  0.0 104.8 %shard_map.82 = bf16[512,512]{1,0:T(8,128)(2,1)} custom-call(bf16[512,512]{1,0:T(8,128)(2,1)} %x_ref.1, f32[3,2048]{1,0:T(4,128)} %gain_hbm.1, bf16[3,256,256]{2,1,0:T(8,128)(2,1)} %wv_ref.1, bf16[3,256,256]{2,1,0:T(8,128)(2,1)} %wg_ref.1, f32[3,31,256]{2,1,0:T(8,128)} %taps_hbm.1, f32[3,256]{1,0:T(4,128)} %lng_hbm.1, f32[3,256]{1,0:T(4,128)} %lnb_hbm.1, ...), custom_call_target="tpu_custom_call" | custom-call | tf_op jit(solution)/shard_map/pallas_call | solution.py:735
  104.9 1.9 %copy.10 = bf16[512,512]{1,0:T(8,128)(2,1)} copy(bf16[512,512]{1,0:T(8,128)(2,1)} %shard_map.82) | data formatting | bytes 1048576

commit v5 on v4

--- a/solution.py
+++ b/solution.py
@@ -49,7 +49,7 @@
 }
 END_PLAN = {
     1: ((O, 0, 0, RISEN), (O, 1, 0, EARLY)), 2: ((O, 2, 0, EARLY), (O, 1, 0, LAST)),
-    3: ((O, 3, 0, EARLY), (XOWN, G, 1), (O, 2, 0, LAST)), 4: ((V, 0, 1), *LAST_Z, (O, 3, 0, LAST)),
+    3: ((O, 3, 0, EARLY), (XOWN, G, 1)), 14: ((O, 2, 0, LAST),), 4: ((V, 0, 1), *LAST_Z, (O, 3, 0, LAST)),
     13: ((G, 0, 1, FIRST), (V, 1, 1, FIRST), (V, 2, 1, FIRST)),
     6: ((V, 1, 1, RISEN),), 7: ((V, 2, 1, RISEN), (SIDE, V, 1)), 8: ((G, 0, 1, RISEN), (SIDE, G, 1)),
     9: ((G, 1, 1),), 10: ((G, 2, 1),), 12: ((XOWN, V, 2),),
@@ -139,10 +139,10 @@
 
     def load_weight(m, l):
         src, dst = ((wv_ref, wv_all), (wg_ref, wg_all))[m]
-        return pltpu.make_async_copy(src.at[l], dst.at[l, own_rows(sp), :], in_sem.at[m, l])
+        return pltpu.make_async_copy(src.at[l], dst.at[l, own_rows(sp), :], in_sem.at[0 if l == 0 else 1])
 
     def load_out(l):
-        return pltpu.make_async_copy(wo_ref.at[l], o_slot(l, inner, tp), in_sem.at[2, l])
+        return pltpu.make_async_copy(wo_ref.at[l], o_slot(l, inner, tp), in_sem.at[2])
 
     def load_rows():
         return pltpu.make_async_copy(x_ref, xf.at[tp, pl.ds(ext, rows), :], small_sem.at[4])
@@ -174,8 +174,10 @@
         xf[tp, 0:ext, :] = jnp.zeros((ext, dblk), jnp.bfloat16)
 
 
-    for m in range(PAIR):
-        load_weight(m, 0).wait()
+    def loaded(block, k):
+        pltpu.make_async_copy(block, block, in_sem.at[k]).wait()
+
+    loaded(wv_all.at[0, pl.ds(0, PAIR * depth), :], 0)
     pl.semaphore_wait(barrier, 2 + n_tp - 1 + near_end + has_slant.astype(jnp.int32))
 
     def parts(c):
@@ -494,7 +496,7 @@
 
     def store_rows(c):
         r = pl.ds(c * CHUNK, CHUNK)
-        return pltpu.make_async_copy(out_all.at[r, :], out_ref.at[r, :], out_sem.at[c])
+        return pltpu.make_async_copy(out_all.at[r, :], out_ref.at[r, :], out_sem.at[0])
 
     def do_half(l, c, q, final):
         for start, size in parts(c):
@@ -560,14 +562,11 @@
     load_rows().wait()
     for c in range(1, n_chunks):
         ag_start(0, c)
-    for l in range(1, layers):
-        for m in range(PAIR):
-            load_weight(m, l).wait()
+    loaded(wv_all.at[pl.ds(1, layers - 1), pl.ds(0, PAIR * depth), :], 1)
 
     @pl.when(outer == tp)
     def _():
-        for l in range(layers):
-            load_out(l).wait()
+        loaded(wo_all.at[:, 0, pl.ds(0, chan), :], 2)
 
     for small in smalls:
         small.wait()
@@ -616,6 +615,7 @@
         do_norm(l, 1)
         slot(3)
         do_norm(l, 2)
+        slot(14)
         do_norm(l, 3)
         slot(4)
         @pl.when(more)
@@ -718,8 +718,7 @@
     def _():
         before_copy().wait_send()
 
-    for c in range(n_chunks):
-        store_rows(c).wait()
+    pltpu.make_async_copy(out_all, out_ref, out_sem.at[0]).wait()
 
 
 def fused_shards(n_sp, n_tp, inputs, norm_gain, w_value, w_gate, conv_taps, ln_gain, ln_bias, w_out):
@@ -768,9 +767,9 @@
             dma((n_chunks,)),
             dma((2, n_chunks)),
             dma((n_chunks,)),
-            dma((3, layers)),
+            dma((3,)),
             dma((5,)),
-            dma((n_chunks,)),
+            dma((1,)),
         ],
         compiler_params=pltpu.CompilerParams(collective_id=0, has_side_effects=True),
     )(

time: 108 us -> 108 us (level)
  no operation moved by 1% of the time
where the time goes in v5:
time: 108 us; the launch traced here: 107 us
  Pallas kernels  105 us (97%)
  local copies, waits for them, and re-layouts  1.87 us (2%)
    pallas_call x1, Pallas kernels, fused_shards(): pl.pallas_call(functools.partial(fused_kernel, n_sp, n_tp, 1e-06), out_sh...  105 us

profile of v5, /device:TPU:3, one launch (start us, length us, event | category | flops | bytes accessed | tf_op | source)
XLA Modules:
  0.0 106.5 jit_solution(14071155042992181051)
XLA Ops:
  0.0 104.6 %shard_map.82 = bf16[512,512]{1,0:T(8,128)(2,1)} custom-call(bf16[512,512]{1,0:T(8,128)(2,1)} %x_ref.1, f32[3,2048]{1,0:T(4,128)} %gain_hbm.1, bf16[3,256,256]{2,1,0:T(8,128)(2,1)} %wv_ref.1, bf16[3,256,256]{2,1,0:T(8,128)(2,1)} %wg_ref.1, f32[3,31,256]{2,1,0:T(8,128)} %taps_hbm.1, f32[3,256]{1,0:T(4,128)} %lng_hbm.1, f32[3,256]{1,0:T(4,128)} %lnb_hbm.1, ...), custom_call_target="tpu_custom_call" | custom-call | tf_op jit(solution)/shard_map/pallas_call | solution.py:734
  104.7 1.9 %copy.10 = bf16[512,512]{1,0:T(8,128)(2,1)} copy(bf16[512,512]{1,0:T(8,128)(2,1)} %shard_map.82) | data formatting | bytes 1048576
